TPU v7x, 512 devices: a whole 4x8x8 slice. The times are simulated.
512 devices in a mesh: sp: 64 (over z, y), dp: 8 (over x, core).
Axes of the slice: x: 4, y: 8, z: 8, core: 2. Of those that a mesh axis runs over, the one named last changes fastest.
Arguments:
- glu_value: bfloat16 [8, 32768, 512], P('dp', 'sp'), may hold values from -6 to 6
- glu_gate: bfloat16 [8, 32768, 512], P('dp', 'sp'), may hold values from -8 to 8
- cotangent: bfloat16 [8, 32768, 2048], P('dp', 'sp'), may hold values from -8 to 8
- conv_weight: float32 [31, 512], replicated, may hold values from -1 to 1
- norm_gain: float32 [512], replicated, may hold values from 0.1 to 1.9
- norm_shift: float32 [512], replicated, may hold values from -3 to 3
- out_weight: bfloat16 [2048, 512], P('dp'), may hold values from -0.25 to 0.25
Outputs:
- grad_value: bfloat16 [8, 32768, 512], P('dp', 'sp')
- grad_gate: bfloat16 [8, 32768, 512], P('dp', 'sp')
- grad_out_weight: float32 [2048, 512], P('dp')
- grad_conv: float32 [31, 512], replicated
- grad_gain: float32 [512], replicated
- grad_shift: float32 [512], replicated
All inputs are finite; a program needn't handle non-finite values.
Results may differ from a plain program's by a relative error of at most 0.003.
Values may be sent and summed in bfloat16 or wider, within the bound.
A program may use at most 64 MiB of HBM per device.

v0:
```python
import functools
import math

import jax
import jax.numpy as jnp
from jax import lax
from jax.sharding import Mesh
from jax.sharding import PartitionSpec as P

SP = ("sp_0", "sp_1")
DP = ("dp_0", "dp_1")
SP_DP = ("sp_0", "sp_1", "dp_0", "dp_1")


epsilon = 1e-06


def from_behind(value, axis, by):
    count = lax.axis_size(axis)
    pairs = [(i, i + by) for i in range(count) if 0 <= i + by < count]
    return lax.ppermute(value, axis, pairs)


def from_everyone(value, axis):
    count = lax.axis_size(axis)
    return lax.all_to_all(
        jnp.broadcast_to(value[None], (count, *value.shape)), axis, 0, 0, tiled=True
    )


def joined_along(pieces, dim):
    pieces = jnp.moveaxis(pieces, 0, dim)
    dims = pieces.shape
    return pieces.reshape(*dims[:dim], dims[dim] * dims[dim + 1], *dims[dim + 2 :])


def whole_of(value, axes, dim):
    far, near = axes
    initial = from_everyone(value, far)
    pieces = jnp.swapaxes(from_everyone(initial, near), 0, 1)
    return joined_along(pieces.reshape(-1, *value.shape), dim)


def over_axes(value, axes):
    return functools.reduce(lax.psum, axes, value)


def cut_along(value, dim, count):
    before, after = (value.shape[:dim], value.shape[dim + 1 :])
    return jnp.moveaxis(value.reshape(*before, count, -1, *after), dim, 0)


def sent_and_summed(value, axis, dim):
    pieces = cut_along(value, dim, lax.axis_size(axis))
    arrived = lax.all_to_all(pieces, axis, split_axis=0, concat_axis=0, tiled=True)
    return arrived.sum(axis=0)


def sum_in_two_steps(value, axes, dim):
    far, near = axes
    own = sent_and_summed(cut_along(value, dim, lax.axis_size(far)), near, dim + 1)
    return jnp.sum(lax.all_to_all(own, far, 0, 0, tiled=True), axis=0)


def rows_for(lines, count):
    spare = -len(lines) % count
    return jnp.pad(lines, [(0, spare)] + [(0, 0)] * (lines.ndim - 1))


def gathered_copies(value, axis, dim):
    return joined_along(from_everyone(value, axis), dim)


def nested_sum(value, axes):
    lines = value.reshape(-1, value.shape[-1])
    padded = rows_for(lines, lax.axis_size(axes))
    whole = gathered_copies(sent_and_summed(padded, axes, 0), axes, 0)
    return lax.slice_in_dim(whole, 0, len(lines)).reshape(value.shape)


def per_device(glu_value, glu_gate, cotangent, conv_weight, norm_gain, norm_shift, out_weight):
    value_rows = glu_value[0]
    gate_rows = glu_gate[0]
    cotan_rows = cotangent[0]
    length = value_rows.shape[0]
    channels = value_rows.shape[1]
    tap_count = conv_weight.shape[0]
    halo_rows = tap_count - 1
    count_sp = lax.axis_size(SP)
    count_dp = lax.axis_size(DP)
    scale = 1.0 / math.sqrt(length * count_sp * count_dp)
    prior_value, prior_gate = from_behind(
        (value_rows[length - halo_rows :], gate_rows[length - halo_rows :]), SP, 1
    )
    value_ext = jnp.concatenate([prior_value, value_rows], axis=0).astype(jnp.float32)
    gate_ext = jnp.concatenate([prior_gate, gate_rows], axis=0).astype(jnp.float32)
    gated_ext = value_ext * jax.nn.sigmoid(gate_ext)
    conv_rows = jnp.zeros((length, channels), jnp.float32)
    for offset in range(tap_count):
        conv_rows = conv_rows + conv_weight[offset] * gated_ext[offset : offset + length]
    centred = conv_rows - jnp.mean(conv_rows, axis=-1, keepdims=True)
    inv_std = lax.rsqrt(jnp.mean(centred * centred, axis=-1, keepdims=True) + epsilon)
    normed = centred * inv_std
    pre_act = normed * norm_gain + norm_shift
    sigmoid_pre = jax.nn.sigmoid(pre_act)
    act_rows = (pre_act * sigmoid_pre).astype(jnp.bfloat16)
    columns = cotan_rows
    grad_act = jnp.dot(
        columns, whole_of(out_weight, ("dp_0", "dp_1"), 0), preferred_element_type=jnp.float32
    )
    grad_pre = grad_act * sigmoid_pre * (1.0 + pre_act * (1.0 - sigmoid_pre))
    grad_normed = grad_pre * norm_gain
    grad_conv_rows = inv_std * (
        grad_normed
        - jnp.mean(grad_normed, axis=-1, keepdims=True)
        - normed * jnp.mean(grad_normed * normed, axis=-1, keepdims=True)
    )
    later_grads = from_behind(grad_conv_rows[:halo_rows], SP, -1)
    padded_grad = jnp.concatenate([grad_conv_rows, later_grads], axis=0)
    grad_gated = jnp.zeros((length, channels), jnp.float32)
    for offset in range(tap_count):
        start = tap_count - 1 - offset
        grad_gated = grad_gated + conv_weight[offset] * padded_grad[start : start + length]
    grad_taps = jnp.stack(
        [
            jnp.sum(grad_conv_rows * gated_ext[offset : offset + length], axis=0)
            for offset in range(tap_count)
        ],
        axis=0,
    )
    sigmoid_gate = jax.nn.sigmoid(gate_ext[halo_rows:])
    grad_value = (grad_gated * sigmoid_gate).astype(jnp.bfloat16)
    grad_gate = (grad_gated * value_ext[halo_rows:] * sigmoid_gate * (1.0 - sigmoid_gate)).astype(
        jnp.bfloat16
    )
    grad_conv, grad_gain, grad_shift = (
        over_axes(grad_taps * scale, SP_DP),
        over_axes(jnp.sum(grad_pre * normed, axis=0) * scale, SP_DP),
        over_axes(jnp.sum(grad_pre, axis=0) * scale, SP_DP),
    )
    columns = cotan_rows
    product = lax.dot_general(
        columns, act_rows, (((0,), (0,)), ((), ())), preferred_element_type=jnp.float32
    )
    partial_rows = sum_in_two_steps(product * scale, ("dp_0", "dp_1"), 0)
    grad_out_weight = nested_sum(partial_rows, SP)
    return (grad_value[None], grad_gate[None], grad_out_weight, grad_conv, grad_gain, grad_shift)


def solution(mesh):
    split = Mesh(mesh.devices.reshape(8, 8, 4, 2), ("sp_0", "sp_1", "dp_0", "dp_1"))
    return jax.shard_map(
        per_device,
        mesh=split,
        in_specs=(P(DP, SP, None), P(DP, SP, None), P(DP, SP, None), P(), P(), P(), P(DP, None)),
        out_specs=(P(DP, SP, None), P(DP, SP, None), P(DP, None), P(), P(), P()),
        check_vma=False,
    )
```

profile of v0, /device:TPU:1, one launch (start us, length us, event | category | flops | bytes accessed | tf_op | source)
XLA Modules:
  0.0 391.4 jit_solution(5961407943740370128)
XLA Ops:
  7.2 0.9 slice_bitcast_fusion
  8.1 4.0 %collective-permute-start.1 = (bf16[30,512]{1,0:T(8,128)(2,1)S(1)}, bf16[30,512]{1,0:T(8,128)(2,1)S(1)}, u32[]{:S(2)}, u32[]{:S(2)}) collective-permute-start(bf16[30,512]{1,0:T(8,128)(2,1)S(1)} %slice_bitcast_fusion), channel_id=1, source_target_pairs={{0,8},{8,16},{16,24},{24,32},{32,40},{40,48},{48,56},{56,64},{64,7... | collective-permute-start | bytes 92168 | tf_op jit(solution)/shard_map/ppermute | solution.py:21
  12.1 0.8 slice_bitcast_fusion.1
  12.9 3.2 collective-permute-start
  16.1 1.1 fusion.114
  17.2 1.1 fusion.115
  18.3 1.6 divide_multiply_fusion
  20.0 5.0 %fusion.113 = (f32[512]{0:T(512)S(1)}, f32[512,512]{1,0:T(8,128)S(1)}) fusion(f32[542,512]{1,0:T(8,128)S(1)} %divide_multiply_fusion, f32[512]{0:T(512)S(1)} %bitcast.158, f32[512]{0:T(512)S(1)} %bitcast.160, f32[512]{0:T(512)S(1)} %bitcast.102, f32[512]{0:T(512)S(1)} %bitcast.104, f32[512]{0:T(512)S(1)} %bitcast.106, f32[512]{0:T(512)S(1)} %bitcast.108, ...), kind=kLoop, calls=%fused_computation.213 | loop fusion | flops 16252416 | bytes 33619968 | tf_op jit(solution)/shard_map/reduce_sum | solution.py:101
  25.2 0.8 copy-done.2
  26.0 3.4 multiply_bitcast_fusion
  29.4 6.6 %reshape_reshape.7 = f32[4,2,256,512]{2,1,0,3:T(2,128)} reshape(f32[2048,512]{0,1:T(8,128)} %multiply_bitcast_fusion) | data formatting | bytes 8388608 | tf_op jit(solution)/shard_map/reshape;reshape | solution.py:50
  36.0 3.3 copy.30
  39.3 10.1 %all_to_all.30 = f32[2,4,256,512]{2,1,3,0:T(4,128)} all-to-all(f32[2,4,256,512]{2,1,3,0:T(4,128)S(1)} %bitcast.94), channel_id=1, replica_groups=mesh['sp_0'=8,'sp_1'=8,'dp_0'=4,'dp_1'=2] {'dp_1'}, dimensions={0} | all-to-all | bytes 8388608 | tf_op jit(solution)/shard_map/all_to_all | solution.py:55
  49.4 1.1 broadcast_in_dim.10
  50.5 4.2 %all-to-all-start = ((bf16[4,256,512]{2,1,0:T(8,128)(2,1)}), bf16[4,256,512]{2,1,0:T(8,128)(2,1)}, u32[]{:S(2)}, u32[]{:S(2)}) async-start(bf16[4,256,512]{2,1,0:T(8,128)(2,1)} %broadcast_in_dim.10), calls=%async_computation | async-start | bytes 2097152 | tf_op jit(solution)/shard_map/all_to_all | solution.py:26
  54.7 5.1 %reduce_sum.364 = f32[4,256,512]{1,0,2:T(4,128)} reduce(f32[2,4,256,512]{2,1,3,0:T(4,128)} %all_to_all.30, f32[]{:T(128)} %constant.5.clone.1), dimensions={0}, to_apply=%region_4.0 | reduce | flops 524288 | bytes 6291460 | tf_op jit(solution)/shard_map/reduce_sum | solution.py:56
  59.8 3.3 copy.24
  63.1 6.5 %all-to-all-done = bf16[4,256,512]{2,1,0:T(8,128)(2,1)} async-done(((bf16[4,256,512]{2,1,0:T(8,128)(2,1)}), bf16[4,256,512]{2,1,0:T(8,128)(2,1)}, u32[]{:S(2)}, u32[]{:S(2)}) %all-to-all-start) | async-done | bytes 1048608 | tf_op jit(solution)/shard_map/all_to_all | solution.py:26
  69.6 1.4 broadcast_in_dim.11
  71.0 7.2 %all_to_all.31 = bf16[2,4,256,512]{3,2,1,0:T(8,128)(2,1)} all-to-all(bf16[2,4,256,512]{3,2,1,0:T(8,128)(2,1)S(1)} %broadcast_in_dim.11), channel_id=1, replica_groups=mesh['sp_0'=8,'sp_1'=8,'dp_0'=4,'dp_1'=2] {'dp_1'}, dimensions={0} | all-to-all | bytes 4194304 | tf_op jit(solution)/shard_map/all_to_all | solution.py:26
  78.2 4.6 %all-to-all-start.3 = ((f32[4,256,512]{1,2,0:T(8,128)}), f32[4,256,512]{1,2,0:T(8,128)}, u32[]{:S(2)}, u32[]{:S(2)}) async-start(f32[4,256,512]{1,2,0:T(8,128)} %copy.24), calls=%async_computation.3 | async-start | bytes 4194304 | tf_op jit(solution)/shard_map/all_to_all | solution.py:62
  82.8 1.9 copy.21
  84.7 1.8 multiply_reduce_fusion
  86.6 3.9 %multiply_reduce_fusion.1 = (f32[512]{0:T(512)S(1)}, f32[512]{0:T(512)S(1)}, f32[512]{0:T(512)S(1)}, f32[512]{0:T(512)S(1)}, f32[512]{0:T(512)S(1)}, /*index=5*/...) fusion(f32[542,512]{1,0:T(8,128)S(1)} %divide_multiply_fusion, ...), kind=kLoop, calls=%fused_computation.153 | loop fusion | flops 11262976 | bytes 22067200 | tf_op jit(solution)/shard_map/reduce_sum | solution.py:126
  90.5 18.2 %all-to-all-done.3 = f32[4,256,512]{1,2,0:T(8,128)} async-done(((f32[4,256,512]{1,2,0:T(8,128)}), f32[4,256,512]{1,2,0:T(8,128)}, u32[]{:S(2)}, u32[]{:S(2)}) %all-to-all-start.3) | async-done | bytes 2097184 | tf_op jit(solution)/shard_map/all_to_all | solution.py:62
  108.8 2.6 reduce_sum.365
  111.3 2.0 copy.26
  113.4 2.0 reshape.45
  115.3 16.0 %all-to-all-start.4 = ((f32[64,4,512]{2,1,0:T(4,128)}), f32[64,4,512]{2,1,0:T(4,128)}, u32[]{:S(2)}, u32[]{:S(2)}) async-start(f32[64,4,512]{2,1,0:T(4,128)} %reshape.45), calls=%async_computation.4 | async-start | bytes 1048576 | tf_op jit(solution)/shard_map/all_to_all | solution.py:55
  131.4 2.7 multiply_reduce_fusion.19
  134.3 0.6 broadcast_multiply_fusion.1
  134.9 0.6 broadcast_multiply_fusion
  135.6 2.2 maximum_convert_fusion.1
  137.9 1.3 collective-permute-start.2
  139.2 67.9 %all-reduce.11.cloned.1.call-done = (f32[31,512]{1,0:T(8,128)}, f32[512]{0:T(512)}, f32[512]{0:T(512)}) async-done(((f32[31,512]{1,0:T(8,128)}, f32[512]{0:T(512)}, f32[512]{0:T(512)}), (f32[31,512]{1,0:T(8,128)}, f32[512]{0:T(512)}, f32[512]{0:T(512)})) %all-reduce.11.cloned.1.call-update) | async-done | bytes 67600 | tf_op jit(solution)/shard_map/psum | solution.py:45
  207.2 2.3 maximum_convert_fusion
  209.4 74.0 %all-reduce.9.cloned.1.call-done = (f32[31,512]{1,0:T(8,128)}, f32[512]{0:T(512)}, f32[512]{0:T(512)}) async-done(((f32[31,512]{1,0:T(8,128)}, f32[512]{0:T(512)}, f32[512]{0:T(512)}), (f32[31,512]{1,0:T(8,128)}, f32[512]{0:T(512)}, f32[512]{0:T(512)})) %all-reduce.9.cloned.1.call-update) | async-done | bytes 67600 | tf_op jit(solution)/shard_map/psum | solution.py:45
  283.5 1.2 reduce_sum.366
  284.6 0.9 broadcast_in_dim.14
  285.5 11.3 %all-to-all-start.5 = ((f32[64,4,512]{2,1,0:T(4,128)}), f32[64,4,512]{2,1,0:T(4,128)}, u32[]{:S(2)}, u32[]{:S(2)}) async-start(f32[64,4,512]{2,1,0:T(4,128)} %broadcast_in_dim.14), calls=%async_computation.5 | async-start | bytes 1048576 | tf_op jit(solution)/shard_map/all_to_all | solution.py:26
  296.8 7.3 %fusion.105 = (bf16[1,512,512]{2,1,0:T(8,128)(2,1)}, f32[512,512]{1,0:T(8,128)}) fusion(f32[542,512]{1,0:T(8,128)} %maximum_convert_fusion, f32[542,512]{1,0:T(8,128)} %maximum_convert_fusion.1, f32[512,512]{1,0:T(8,128)S(1)} %copy-done.1, f32[512]{0:T(512)S(1)} %bitcast.159, f32[30,512]{1,0:T(8,128)S(1)} %collective-permute-done.2, f32[512]{0:T(512)S(1)} %bitcast.161, ...), kind=kLoop, calls=%fused_computation.197 | loop fusion | flops 25952256 | bytes 4843520 | tf_op jit(solution)/shard_map/broadcast_in_dim | solution.py:147
  304.1 35.2 %all-reduce.13.cloned.1.call-done = (f32[31,512]{1,0:T(8,128)}, f32[512]{0:T(512)}, f32[512]{0:T(512)}) async-done(((f32[31,512]{1,0:T(8,128)}, f32[512]{0:T(512)}, f32[512]{0:T(512)}), (f32[31,512]{1,0:T(8,128)}, f32[512]{0:T(512)}, f32[512]{0:T(512)})) %all-reduce.13.cloned.1.call-update) | async-done | bytes 67600 | tf_op jit(solution)/shard_map/psum | solution.py:45
  339.3 2.6 fusion.104
  341.9 2.0 reshape.46
  344.0 36.9 %all-reduce.15.cloned.1.call-done = (f32[31,512]{1,0:T(8,128)}, f32[512]{0:T(512)}, f32[512]{0:T(512)}) async-done(((f32[31,512]{1,0:T(8,128)}, f32[512]{0:T(512)}, f32[512]{0:T(512)}), (f32[31,512]{1,0:T(8,128)}, f32[512]{0:T(512)}, f32[512]{0:T(512)})) %all-reduce.15.cloned.1.call-update) | async-done | bytes 67600 | tf_op jit(solution)/shard_map/psum | solution.py:45
  380.9 1.5 copy.43
  382.4 1.2 copy.44
  383.6 1.2 copy.45
  (32 shorter events, 0.7 us)
Async XLA Ops:
  7.2 18.9 %copy-start = (bf16[1,512,2048]{2,1,0:T(8,128)(2,1)S(1)}, bf16[1,512,2048]{2,1,0:T(8,128)(2,1)}, u32[]{:S(2)}) copy-start(bf16[1,512,2048]{2,1,0:T(8,128)(2,1)} %param.9) | copy-start | bytes 6291460
  8.1 10.2 %collective-permute-start.1 = (bf16[30,512]{1,0:T(8,128)(2,1)S(1)}, bf16[30,512]{1,0:T(8,128)(2,1)S(1)}, u32[]{:S(2)}, u32[]{:S(2)}) collective-permute-start(bf16[30,512]{1,0:T(8,128)(2,1)S(1)} %slice_bitcast_fusion), channel_id=1, source_target_pairs={{0,8},{8,16},{16,24},{24,32},{32,40},{40,48},{48,56},{56,64},{64,7... | collective-permute-start | bytes 92168 | tf_op jit(solution)/shard_map/ppermute | solution.py:21
  12.9 5.4 %collective-permute-start = (bf16[30,512]{1,0:T(8,128)(2,1)S(1)}, bf16[30,512]{1,0:T(8,128)(2,1)S(1)}, u32[]{:S(2)}, u32[]{:S(2)}) collective-permute-start(bf16[30,512]{1,0:T(8,128)(2,1)S(1)} %slice_bitcast_fusion.1), channel_id=1, source_target_pairs={{0,8},{8,16},{16,24},{24,32},{32,40},{40,48},{48,56},{56,64},{64,7... | collective-permute-start | bytes 92168 | tf_op jit(solution)/shard_map/ppermute | solution.py:21
  19.9 6.1 %copy-start.5 = (f32[512]{0:T(512)S(1)}, f32[512]{0:T(512)}, u32[]{:S(2)}) copy-start(f32[512]{0:T(512)} %param.11) | copy-start | bytes 6148
  19.9 6.1 %copy-start.6 = (f32[512]{0:T(512)S(1)}, f32[512]{0:T(512)}, u32[]{:S(2)}) copy-start(f32[512]{0:T(512)} %param.12) | copy-start | bytes 6148
  24.9 1.1 copy-start.2
  39.3 10.1 %copy-start.4 = (bf16[256,512]{1,0:T(8,128)(2,1)S(1)}, bf16[256,512]{1,0:T(8,128)(2,1)}, u32[]{:S(2)}) copy-start(bf16[256,512]{1,0:T(8,128)(2,1)} %param.13) | copy-start | bytes 786436
  50.5 19.1 %all-to-all-start = ((bf16[4,256,512]{2,1,0:T(8,128)(2,1)}), bf16[4,256,512]{2,1,0:T(8,128)(2,1)}, u32[]{:S(2)}, u32[]{:S(2)}) async-start(bf16[4,256,512]{2,1,0:T(8,128)(2,1)} %broadcast_in_dim.10), calls=%async_computation | async-start | bytes 2097152 | tf_op jit(solution)/shard_map/all_to_all | solution.py:26
  78.2 30.6 %all-to-all-start.3 = ((f32[4,256,512]{1,2,0:T(8,128)}), f32[4,256,512]{1,2,0:T(8,128)}, u32[]{:S(2)}, u32[]{:S(2)}) async-start(f32[4,256,512]{1,2,0:T(8,128)} %copy.24), calls=%async_computation.3 | async-start | bytes 4194304 | tf_op jit(solution)/shard_map/all_to_all | solution.py:62
  82.8 1.9 copy-start.3
  115.3 168.1 %all-to-all-start.4 = ((f32[64,4,512]{2,1,0:T(4,128)}), f32[64,4,512]{2,1,0:T(4,128)}, u32[]{:S(2)}, u32[]{:S(2)}) async-start(f32[64,4,512]{2,1,0:T(4,128)} %reshape.45), calls=%async_computation.4 | async-start | bytes 1048576 | tf_op jit(solution)/shard_map/all_to_all | solution.py:55
  131.4 75.7 %all-reduce.11.cloned.1.call-start = ((), (), s32[]{:S(2)}) async-start(), calls=%async_computation.7 | async-start | bytes 139264 | tf_op jit(solution)/shard_map/psum | solution.py:45
  134.2 3.7 copy-start.1
  135.6 147.8 %all-reduce.9.cloned.1.call-start = ((), (), s32[]{:S(2)}) async-start(), calls=%async_computation.6 | async-start | bytes 139264 | tf_op jit(solution)/shard_map/psum | solution.py:45
  137.9 159.0 %collective-permute-start.2 = (f32[30,512]{1,0:T(8,128)S(1)}, f32[30,512]{1,0:T(8,128)S(1)}, u32[]{:S(2)}, u32[]{:S(2)}) collective-permute-start(f32[30,512]{1,0:T(8,128)S(1)} %slice.489), channel_id=1, source_target_pairs={{8,0},{16,8},{24,16},{32,24},{40,32},{48,40},{56,48},{64,56},{72,6... | collective-permute-start | bytes 184328 | tf_op jit(solution)/shard_map/ppermute | solution.py:21
  207.1 132.2 %all-reduce.13.cloned.1.call-start = ((), (), s32[]{:S(2)}) async-start(), calls=%async_computation.8 | async-start | bytes 139264 | tf_op jit(solution)/shard_map/psum | solution.py:45
  285.5 56.5 %all-to-all-start.5 = ((f32[64,4,512]{2,1,0:T(4,128)}), f32[64,4,512]{2,1,0:T(4,128)}, u32[]{:S(2)}, u32[]{:S(2)}) async-start(f32[64,4,512]{2,1,0:T(4,128)} %broadcast_in_dim.14), calls=%async_computation.5 | async-start | bytes 1048576 | tf_op jit(solution)/shard_map/all_to_all | solution.py:26
  296.8 84.1 %all-reduce.15.cloned.1.call-start = ((), (), s32[]{:S(2)}) async-start(), calls=%async_computation.9 | async-start | bytes 139264 | tf_op jit(solution)/shard_map/psum | solution.py:45
Sparse Core Ops, SparseCore 0:
  135.7 71.3 all-reduce.10
  209.6 73.7 all-reduce.8
  285.9 53.3 all-reduce.12
  342.1 38.6 all-reduce.14
where the time goes:
time: 393 us; the launch traced here: 391 us
  waiting for transfers between devices  239 us (61%)
  starting transfers between devices  44.9 us (11%)
  other arithmetic  37.9 us (10%)
  local copies, waits for them, and re-layouts  33.2 us (8%)
  blocking collectives  17.3 us (4%)
  between operations  14 us (4%)
  matrix products  5.23 us (1%)
    psum x4, waiting for transfers between devices, over_axes(): return functools.reduce(lax.psum, axes, value)  214 us
    all_to_all x1, waiting for transfers between devices, sum_in_two_steps(): return jnp.sum(lax.all_to_all(own, far, 0, 0, tiled=True), axis=0)  18.2 us
    all_to_all x1, starting transfers between devices, sent_and_summed(): lax.all_to_all(pieces, axis, split_axis=0, concat_axis=0, tiled=True)  16 us
    all_to_all x2, starting transfers between devices, from_everyone(): lax.all_to_all(jnp.broadcast_to(value[None], (count, *value.shape)), axis...  15.5 us
    all_to_all x1, blocking collectives, sent_and_summed(): lax.all_to_all(pieces, axis, split_axis=0, concat_axis=0, tiled=True)  10.1 us
    another operation x2, local copies, waits for them, and re-layouts, cut_along(): return jnp.moveaxis(value.reshape(*before, count, -1, *after), dim, 0)  9.84 us
    ppermute x3, starting transfers between devices, from_behind(): return lax.ppermute(value, axis, pairs)  8.52 us
  transfers between devices with their start and end apart: 11, of which 6 were waited for; matrix products, arithmetic and copies ran while one was open for 11% of the time, Pallas kernels for 0%

commit v1 on v0

v1 whole, which is shorter than its diff:
```python
import functools
import math

import jax
import jax.numpy as jnp
from jax import lax
from jax.experimental import pallas as pl
from jax.experimental.pallas import tpu as pltpu
from jax.sharding import PartitionSpec as P

MESH = pl.DeviceIdType.MESH
F32 = jnp.float32
BF16 = jnp.bfloat16

EPS = 1e-06
LANES = 128
HALO = 32
TILE = 64
SIDE = 8
CHIPS = 4
SMALL = 40
N_COPIES = 128


def sigmoid(x):
    return jax.nn.sigmoid(x)


def dot_t(a, b):
    return lax.dot_general(a, b, (((0,), (0,)), ((), ())), preferred_element_type=F32)


def kernel(
    scale, v_ref, g_ref, cot_ref, w_ref, gain_ref, shift_ref, ow_ref,
    gv_ref, gg_ref, gw_ref, sm_out,
    hv, hg, gated, normed, invs, dsil, ga, gcr, act, actp, cotp, wfull,
    stage, recvx, gsum, st_a, st_b, rs_a, rs_b, t_a, t_b, rt_a, rt_b, fin_a, fin_b,
    taps, acc_gs, sm_own, sm_par, sm_x, sm_2, sm_y, sm_z, sm_f,
    send_sems, recv_sems,
):
    rows, channels = v_ref.shape
    n_taps = w_ref.shape[0]
    blocks = channels // LANES
    features = ow_ref.shape[0]
    sp = lax.axis_index("sp")
    dp = lax.axis_index("dp")
    n_sp = SIDE * SIDE
    z, y = sp // SIDE, sp % SIDE
    x, core = dp // 2, dp % 2
    me_partner = {"sp": sp, "dp": 2 * x + (1 - core)}

    def at_x(k):
        return {"sp": sp, "dp": 2 * ((x + k) % CHIPS) + core}

    def at_y(k):
        return {"sp": z * SIDE + (y + k) % SIDE, "dp": dp}

    def at_z(k):
        return {"sp": ((z + k) % SIDE) * SIDE + y, "dp": dp}

    after = {"sp": (sp + 1) % n_sp, "dp": dp}
    before = {"sp": (sp + n_sp - 1) % n_sp, "dp": dp}

    counter = [0]
    started = []

    def send(src, dst, device):
        i = counter[0]
        counter[0] += 1
        copy = pltpu.make_async_remote_copy(
            src_ref=src, dst_ref=dst, send_sem=send_sems.at[i], recv_sem=recv_sems.at[i],
            device_id=device, device_id_type=MESH,
        )
        copy.start()
        started.append(copy)
        return copy

    barrier = pltpu.get_barrier_semaphore()
    peers = [me_partner, after, before]
    peers += [at_x(k) for k in range(1, CHIPS)]
    peers += [at_y(k) for k in range(1, SIDE)]
    peers += [at_z(k) for k in range(1, SIDE)]
    for peer in peers:
        pl.semaphore_signal(barrier, inc=1, device_id=peer, device_id_type=MESH)

    def lanes(cb):
        return slice(cb * LANES, (cb + 1) * LANES)

    def gate_tile(i, _):
        base = pl.multiple_of(i * TILE, TILE)
        for cb in range(blocks):
            v = v_ref[pl.ds(base, TILE), lanes(cb)].astype(F32)
            g = g_ref[pl.ds(base, TILE), lanes(cb)].astype(F32)
            gated[cb, pl.ds(base + HALO, TILE), :] = v * sigmoid(g)
        return 0

    lax.fori_loop(0, rows // TILE, gate_tile, 0)
    pl.semaphore_wait(barrier, len(peers))

    halo_v = send(v_ref.at[pl.ds(rows - HALO, HALO), :], hv, after)
    halo_g = send(g_ref.at[pl.ds(rows - HALO, HALO), :], hg, after)

    def shard(owner_x, owner_core):
        start = pl.multiple_of((2 * owner_x + owner_core) * features, features)
        return wfull.at[pl.ds(start, features), :]

    own_shard = shard(x, core)
    to_right = send(ow_ref, own_shard, at_x(1))
    to_left = send(ow_ref, own_shard, at_x(CHIPS - 1))
    to_other = send(ow_ref, own_shard, me_partner)

    def columns(owner_x, owner_core):
        return pl.ds(pl.multiple_of((2 * owner_x + owner_core) * features, features), features)

    cot_copies = [
        send(cot_ref.at[:, columns(k, 1 - core)], cotp.at[k], me_partner) for k in range(CHIPS)
    ]
    start = pl.multiple_of(dp * features, features)
    wfull[pl.ds(start, features), :] = ow_ref[...]

    def forward_tile(base):
        conv = []
        for cb in range(blocks):
            acc = jnp.zeros((TILE, LANES), F32)
            for j in range(n_taps):
                tap = w_ref[j : j + 1, lanes(cb)]
                acc = acc + tap * gated[cb, pl.ds(base + (j + HALO - n_taps + 1), TILE), :]
            conv.append(acc)
        total = functools.reduce(lambda a, b: a + b, conv)
        mean = jnp.sum(total, axis=-1, keepdims=True) * (1.0 / channels)
        centred = [c - mean for c in conv]
        squares = functools.reduce(lambda a, b: a + b, [c * c for c in centred])
        var = jnp.sum(squares, axis=-1, keepdims=True) * (1.0 / channels)
        inv = lax.rsqrt(var + EPS)
        invs[pl.ds(base, TILE), :] = jnp.broadcast_to(inv, (TILE, LANES))
        for cb in range(blocks):
            nrm = centred[cb] * inv
            pre = nrm * gain_ref[0:1, lanes(cb)] + shift_ref[0:1, lanes(cb)]
            sig = sigmoid(pre)
            normed[cb, pl.ds(base, TILE), :] = nrm
            act[pl.ds(base, TILE), lanes(cb)] = (pre * sig).astype(BF16)
            dsil[cb, pl.ds(base, TILE), :] = sig * (1.0 + pre * (1.0 - sig))

    def forward_step(i, _):
        forward_tile(pl.multiple_of(i * TILE, TILE))
        return 0

    lax.fori_loop(1, rows // TILE, forward_step, 0)
    halo_v.wait_recv()
    halo_g.wait_recv()
    inside = (sp > 0).astype(F32)
    for cb in range(blocks):
        v = hv[:, lanes(cb)].astype(F32)
        g = hg[:, lanes(cb)].astype(F32)
        gated[cb, pl.ds(0, HALO), :] = v * sigmoid(g) * inside
    lax.fori_loop(0, 1, forward_step, 0)
    act_copy = send(act, actp, me_partner)

    to_right.wait_recv()
    to_left.wait_recv()
    left_x, right_x = (x + CHIPS - 1) % CHIPS, (x + 1) % CHIPS
    pass_left = send(shard(left_x, core), shard(left_x, core), me_partner)
    pass_right = send(shard(right_x, core), shard(right_x, core), me_partner)
    source_x = (x + CHIPS - 1 + 2 * core) % CHIPS
    target_x = (x + 1 + 2 * core) % CHIPS
    pass_far = send(
        shard(source_x, core), shard(source_x, core), {"sp": sp, "dp": 2 * target_x + core}
    )

    for copy in cot_copies:
        copy.wait_recv()
    act_copy.wait_recv()
    x_copies = []
    for k in (2, 1, 3, 0):
        xt = (x + k) % CHIPS
        product = dot_t(cot_ref[:, columns(xt, core)], act[...]) + dot_t(cotp[xt], actp[...])
        if k:
            stage[k - 1] = product.astype(BF16)
            x_copies.append(send(stage.at[k - 1], recvx.at[k - 1], at_x(k)))
        else:
            gsum[...] = product

    pass_far.wait_recv()
    far_x = (x + 2) % CHIPS
    far_other = send(shard(far_x, core), shard(far_x, core), me_partner)
    to_other.wait_recv()
    pass_left.wait_recv()
    pass_right.wait_recv()
    far_other.wait_recv()

    half = rows // 2

    def matmul_step(i, _):
        base = pl.multiple_of(i * half, half)
        ga[pl.ds(base, half), :] = jnp.dot(
            cot_ref[pl.ds(base, half), :], wfull[...], preferred_element_type=F32
        )
        return 0

    lax.fori_loop(0, 2, matmul_step, 0)

    acc_gs[...] = jnp.zeros_like(acc_gs)
    taps[...] = jnp.zeros_like(taps)

    def fold(a):
        return a.reshape(TILE // 8, 8, LANES).sum(axis=0)

    def grad_step(i, _):
        base = pl.multiple_of(i * TILE, TILE)
        grads, norms = [], []
        for cb in range(blocks):
            gpre = ga[pl.ds(base, TILE), lanes(cb)] * dsil[cb, pl.ds(base, TILE), :]
            nrm = normed[cb, pl.ds(base, TILE), :]
            acc_gs[0, cb] = acc_gs[0, cb] + fold(gpre * nrm)
            acc_gs[1, cb] = acc_gs[1, cb] + fold(gpre)
            grads.append(gpre * gain_ref[0:1, lanes(cb)])
            norms.append(nrm)
        total = functools.reduce(lambda a, b: a + b, grads)
        mean = jnp.sum(total, axis=-1, keepdims=True) * (1.0 / channels)
        along = functools.reduce(lambda a, b: a + b, [a * b for a, b in zip(grads, norms)])
        mean_along = jnp.sum(along, axis=-1, keepdims=True) * (1.0 / channels)
        inv = invs[pl.ds(base, TILE), :]
        for cb in range(blocks):
            gcr[cb, pl.ds(base, TILE), :] = inv * (grads[cb] - mean - norms[cb] * mean_along)
        return 0

    lax.fori_loop(0, 1, grad_step, 0)
    halo_c = send(gcr.at[:, pl.ds(0, HALO), :], gcr.at[:, pl.ds(rows, HALO), :], before)
    lax.fori_loop(1, rows // TILE, grad_step, 0)

    def backward_step(i, _):
        base = pl.multiple_of(i * TILE, TILE)
        for cb in range(blocks):
            acc = jnp.zeros((TILE, LANES), F32)
            own = gated[cb, pl.ds(base + HALO, TILE), :]
            for j in range(n_taps):
                shifted = gcr[cb, pl.ds(base + j, TILE), :]
                acc = acc + w_ref[n_taps - 1 - j : n_taps - j, lanes(cb)] * shifted
                taps[cb, n_taps - 1 - j] = taps[cb, n_taps - 1 - j] + fold(own * shifted)
            v = v_ref[pl.ds(base, TILE), lanes(cb)].astype(F32)
            sig = sigmoid(g_ref[pl.ds(base, TILE), lanes(cb)].astype(F32))
            gs = acc * sig
            gv_ref[pl.ds(base, TILE), lanes(cb)] = gs.astype(BF16)
            gg_ref[pl.ds(base, TILE), lanes(cb)] = (gs * v * (1.0 - sig)).astype(BF16)
        return 0

    middle = rows // TILE // 2
    lax.fori_loop(0, middle, backward_step, 0)

    for copy in x_copies:
        copy.wait_recv()
    part = features // SIDE
    width = channels // 2
    for r in range(SIDE):
        piece = pl.ds(r * part, part)
        total = gsum[piece, :]
        for k in range(CHIPS - 1):
            total = total + recvx[k, piece, :].astype(F32)
        gsum[piece, :] = total
        st_a[r] = total[:, :width].astype(BF16)
        st_b[r] = total[:, width:].astype(BF16)
    order = (4, 3, 5, 2, 6, 1, 7)
    first_a, first_b = [], []
    for k in order:
        first_a.append(send(st_a.at[(y + k) % SIDE], rs_a.at[k - 1], at_y(k)))
        first_b.append(send(st_b.at[(z + k) % SIDE], rs_b.at[k - 1], at_z(k)))

    halo_c.wait_recv()
    beyond = (sp < n_sp - 1).astype(F32)
    for cb in range(blocks):
        gcr[cb, pl.ds(rows, HALO), :] = gcr[cb, pl.ds(rows, HALO), :] * beyond
    lax.fori_loop(middle, rows // TILE, backward_step, 0)

    per_block = SMALL // 8
    row_ids = lax.broadcasted_iota(jnp.int32, (8, LANES), 0)
    for t in range(24):
        cb, rb = t // per_block, t % per_block
        tile = jnp.zeros((8, LANES), F32)
        if cb < blocks:
            for r in range(8):
                j = rb * 8 + r
                if j < n_taps:
                    line = taps[cb, j]
                elif j < n_taps + 2:
                    line = acc_gs[j - n_taps, cb]
                else:
                    continue
                line = jnp.sum(line, axis=0, keepdims=True) * scale
                tile = jnp.where(row_ids == r, line, tile)
        sm_own[t // 3, t % 3] = tile
    small_other = send(sm_own, sm_par, me_partner)

    for copy in first_a + first_b:
        copy.wait_recv()

    def first_sum(own_index, rs, column, t_ref):
        total = gsum[pl.ds(pl.multiple_of(own_index * part, part), part), pl.ds(column, width)]
        for k in range(SIDE - 1):
            total = total + rs[k].astype(F32)
        total = total * scale
        for t in range(SIDE):
            r, c = t // 2, t % 2
            t_ref[t] = total[r * 8 : r * 8 + 8, c * LANES : (c + 1) * LANES]

    first_sum(y, rs_a, 0, t_a)
    first_sum(z, rs_b, width, t_b)
    second_a, second_b = [], []
    for k in order:
        second_a.append(send(t_a.at[(z + k) % SIDE], rt_a.at[k - 1], at_z(k)))
        second_b.append(send(t_b.at[(y + k) % SIDE], rt_b.at[k - 1], at_y(k)))

    small_other.wait_recv()
    sm_x[x] = sm_own[...] + sm_par[...]
    small_x = [send(sm_x.at[x], sm_x.at[x], at_x(k)) for k in (2, 1, 3)]

    for copy in second_a + second_b:
        copy.wait_recv()
    final_a, final_b = t_a[z], t_b[y]
    for k in range(SIDE - 1):
        final_a = final_a + rt_a[k]
        final_b = final_b + rt_b[k]
    fin_a[y, z] = final_a
    fin_b[z, y] = final_b
    spread_a, spread_b = [], []
    for k in order:
        spread_a.append(send(fin_a.at[y, z], fin_a.at[y, z], at_z(k)))
        spread_b.append(send(fin_b.at[z, y], fin_b.at[z, y], at_y(k)))

    for copy in small_x:
        copy.wait_recv()
    total = sm_x[0]
    for k in range(1, CHIPS):
        total = total + sm_x[k]
    sm_2[...] = total
    sm_y[y] = sm_2[y]
    small_y = [send(sm_2.at[(y + k) % SIDE], sm_y.at[y], at_y(k)) for k in order]

    for copy in spread_a + spread_b:
        copy.wait_recv()
    last_a, last_b = [], []
    for k in order:
        last_a.append(send(fin_a.at[y], fin_a.at[y], at_y(k)))
        last_b.append(send(fin_b.at[z], fin_b.at[z], at_z(k)))

    for copy in small_y:
        copy.wait_recv()
    total = sm_y[0]
    for k in range(1, SIDE):
        total = total + sm_y[k]
    sm_z[z] = total
    small_z = [send(sm_z.at[z], sm_z.at[z], at_z(k)) for k in order]
    for copy in small_z:
        copy.wait_recv()
    total = sm_z[0]
    for k in range(1, SIDE):
        total = total + sm_z[k]
    sm_f[y] = total
    small_f = [send(sm_f.at[y], sm_f.at[y], at_y(k)) for k in order]

    for copy in last_a + last_b:
        copy.wait_recv()
    for r in range(SIDE):
        for t in range(SIDE):
            line = slice(r * part + (t // 2) * 8, r * part + (t // 2) * 8 + 8)
            c = (t % 2) * LANES
            gw_ref[line, c : c + LANES] = fin_a[r, t]
            gw_ref[line, width + c : width + c + LANES] = fin_b[r, t]

    for copy in small_f:
        copy.wait_recv()
    for t in range(blocks * per_block):
        cb, rb = t // per_block, t % per_block
        sm_out[rb * 8 : rb * 8 + 8, lanes(cb)] = sm_f[t // 3, t % 3]
    for copy in started:
        copy.wait_send()


def per_device(count, glu_value, glu_gate, cotangent, conv_weight, norm_gain, norm_shift, out_weight):
    value, gate, cot = glu_value[0], glu_gate[0], cotangent[0]
    rows, channels = value.shape
    n_taps = conv_weight.shape[0]
    features = out_weight.shape[0]
    blocks = channels // LANES
    part, width = features // SIDE, channels // 2
    scale = 1.0 / math.sqrt(rows * count)
    vmem = pl.BlockSpec(memory_space=pltpu.VMEM)
    shape = jax.ShapeDtypeStruct
    tile = (8, LANES)
    small = (SIDE, 3, *tile)
    outs = pl.pallas_call(
        functools.partial(kernel, scale),
        out_shape=[
            shape((rows, channels), BF16),
            shape((rows, channels), BF16),
            shape((features, channels), F32),
            shape((SMALL, channels), F32),
        ],
        in_specs=[vmem] * 7,
        out_specs=[vmem] * 4,
        scratch_shapes=[
            pltpu.VMEM((HALO, channels), BF16),
            pltpu.VMEM((HALO, channels), BF16),
            pltpu.VMEM((blocks, rows + HALO, LANES), F32),
            pltpu.VMEM((blocks, rows, LANES), F32),
            pltpu.VMEM((rows, LANES), F32),
            pltpu.VMEM((blocks, rows, LANES), F32),
            pltpu.VMEM((rows, channels), F32),
            pltpu.VMEM((blocks, rows + HALO, LANES), F32),
            pltpu.VMEM((rows, channels), BF16),
            pltpu.VMEM((rows, channels), BF16),
            pltpu.VMEM((CHIPS, rows, features), BF16),
            pltpu.VMEM((2 * CHIPS * features, channels), BF16),
            pltpu.VMEM((CHIPS - 1, features, channels), BF16),
            pltpu.VMEM((CHIPS - 1, features, channels), BF16),
            pltpu.VMEM((features, channels), F32),
            pltpu.VMEM((SIDE, part, width), BF16),
            pltpu.VMEM((SIDE, part, width), BF16),
            pltpu.VMEM((SIDE - 1, part, width), BF16),
            pltpu.VMEM((SIDE - 1, part, width), BF16),
            pltpu.VMEM((SIDE, *tile), F32),
            pltpu.VMEM((SIDE, *tile), F32),
            pltpu.VMEM((SIDE - 1, *tile), F32),
            pltpu.VMEM((SIDE - 1, *tile), F32),
            pltpu.VMEM((SIDE, SIDE, *tile), F32),
            pltpu.VMEM((SIDE, SIDE, *tile), F32),
            pltpu.VMEM((blocks, n_taps, *tile), F32),
            pltpu.VMEM((2, blocks, *tile), F32),
            pltpu.VMEM(small, F32),
            pltpu.VMEM(small, F32),
            pltpu.VMEM((CHIPS, *small), F32),
            pltpu.VMEM(small, F32),
            pltpu.VMEM(small, F32),
            pltpu.VMEM(small, F32),
            pltpu.VMEM(small, F32),
            pltpu.SemaphoreType.DMA((N_COPIES,)),
            pltpu.SemaphoreType.DMA((N_COPIES,)),
        ],
        compiler_params=pltpu.CompilerParams(
            collective_id=0, has_side_effects=True, vmem_limit_bytes=60 * 2**20
        ),
        name="backward",
    )(value, gate, cot, conv_weight, norm_gain[None], norm_shift[None], out_weight)
    grad_value, grad_gate, grad_weight, lines = outs
    return (
        grad_value[None],
        grad_gate[None],
        grad_weight,
        lines[:n_taps],
        lines[n_taps],
        lines[n_taps + 1],
    )


def solution(mesh):
    return jax.shard_map(
        functools.partial(per_device, mesh.size),
        mesh=mesh,
        in_specs=(
            P("dp", "sp", None), P("dp", "sp", None), P("dp", "sp", None),
            P(), P(), P(), P("dp", None),
        ),
        out_specs=(P("dp", "sp", None), P("dp", "sp", None), P("dp", None), P(), P(), P()),
        check_vma=False,
    )
```

time: 393 us -> 82.4 us (0.21)
  waiting for transfers between devices: 239 us -> 0 us
  Pallas kernels: 0 us -> 74.1 us
  starting transfers between devices: 44.9 us -> 0 us
  other arithmetic: 37.9 us -> 0 us
  local copies, waits for them, and re-layouts: 33.2 us -> 7.38 us
  blocking collectives: 17.3 us -> 0 us
  between operations: 14 us -> 0.65 us
  matrix products: 5.23 us -> 0 us
    psum x4 -> x0, waiting for transfers between devices: 214 us -> none  [over_axes(): return functools.reduce(lax.psum, axes, value)]
    pallas_call x0 -> x1, Pallas kernels: none -> 74.1 us  [per_device(): pl.pallas_call(functools.partial(kernel, scale), out_shape=[shape((rows,...]
    all_to_all x4 -> x0, starting transfers between devices: 36.2 us -> none  [the longest x1 16 us: sent_and_summed(): lax.all_to_all(pieces, axis, split_axis=0, concat_axis=0, tiled=True)]
    all_to_all x4 -> x0, waiting for transfers between devices: 24.7 us -> none  [the longest x1 18.2 us: sum_in_two_steps(): return jnp.sum(lax.all_to_all(own, far, 0, 0, tiled=True), axis=0)]
    reduce_sum x7 -> x0, other arithmetic: 20.7 us -> none  [the longest x2 6.7 us: per_device(): jnp.sum(grad_conv_rows * gated_ext[offset:offset + length], axis=0)]
    all_to_all x2 -> x0, blocking collectives: 17.3 us -> none  [the longest x1 10.1 us: sent_and_summed(): lax.all_to_all(pieces, axis, split_axis=0, concat_axis=0, tiled=True)]
    another operation x3 -> x0, local copies, waits for them, and re-layouts: 9.99 us -> none  [the longest x2 9.84 us: cut_along(): return jnp.moveaxis(value.reshape(*before, count, -1, *after), dim, 0)]
    broadcast_in_dim x2 -> x0, other arithmetic: 9.9 us -> none  [the longest x1 7.28 us: per_device(): grad_gate[None]]
  transfers between devices with their start and end apart: 11 -> 0, of which waited for: 6 -> 0; matrix products, arithmetic and copies ran while one was open for 11% -> 0% of each run, Pallas kernels for 0% -> 0%
where the time goes in v1:
time: 82.4 us; the launch traced here: 82.1 us
  Pallas kernels  74.1 us (90%)
  local copies, waits for them, and re-layouts  7.38 us (9%)
    pallas_call x1, Pallas kernels, per_device(): pl.pallas_call(functools.partial(kernel, scale), out_shape=[shape((rows,...  74.1 us
    unnamed x5, local copies, waits for them, and re-layouts  4.53 us

profile of v1, /device:TPU:1, one launch (start us, length us, event | category | flops | bytes accessed | tf_op | source)
XLA Modules:
  0.0 82.1 jit_solution(16749573594606580478)
XLA Ops:
  0.6 74.1 %backward.1 = (bf16[512,512]{1,0:T(8,128)(2,1)}, bf16[512,512]{1,0:T(8,128)(2,1)}, f32[256,512]{1,0:T(8,128)}, f32[40,512]{1,0:T(8,128)}) custom-call(bf16[512,512]{1,0:T(8,128)(2,1)} %bitcast.12, bf16[512,512]{1,0:T(8,128)(2,1)} %bitcast.13, bf16[512,2048]{1,0:T(8,128)(2,1)} %bitcast.9, f32[31,512]{1,0:T(8,128)} %w_ref.1, f32[1,512]{1,0:T(1,128)} %bitcast.16, ...), custom_call_target="tpu_custom_call" | custom-call | tf_op jit(solution)/shard_map/backward/pallas_call | solution.py:390
  74.7 0.0 copy-start
  74.7 1.4 %fusion = (f32[1,512]{1,0:T(1,128)}, f32[1,512]{1,0:T(1,128)}) fusion(f32[40,512]{1,0:T(8,128)} %get-tuple-element.13), kind=kLoop, calls=%fused_computation | loop fusion | bytes 8192 | tf_op jit(solution)/shard_map/slice | solution.py:450
  76.1 1.5 %slice.9 = f32[31,512]{1,0:T(8,128)} slice(f32[40,512]{1,0:T(8,128)} %get-tuple-element.13), slice={[0:31], [0:512]} | slice | bytes 126976 | tf_op jit(solution)/shard_map/slice | solution.py:448
  77.6 1.9 %copy.16 = bf16[1,512,512]{2,1,0:T(8,128)(2,1)} copy(bf16[1,512,512]{2,1,0:T(8,128)(2,1)} %bitcast.11) | data formatting | bytes 1048576
  79.4 1.9 %copy.17 = bf16[1,512,512]{2,1,0:T(8,128)(2,1)} copy(bf16[1,512,512]{2,1,0:T(8,128)(2,1)} %bitcast.10) | data formatting | bytes 1048576
  81.3 0.0 copy-done
  81.3 0.8 copy.18
Async XLA Ops:
  74.7 6.6 %copy-start = (f32[256,512]{1,0:T(8,128)S(1)}, f32[256,512]{1,0:T(8,128)}, u32[]{:S(2)}) copy-start(f32[256,512]{1,0:T(8,128)} %get-tuple-element.24) | copy-start | bytes 1572868

commit v2 on v1

v2 whole, which is shorter than its diff:
```python
import functools
import math

import jax
import jax.numpy as jnp
from jax import lax
from jax.experimental import pallas as pl
from jax.experimental.pallas import tpu as pltpu
from jax.sharding import PartitionSpec as P

MESH = pl.DeviceIdType.MESH
F32 = jnp.float32
BF16 = jnp.bfloat16

EPS = 1e-06
LANES = 128
HALO = 32
TILE = 64
SIDE = 8
CHIPS = 4
COPIES = 160
SMALL = 40
OWN_TILES = 3
ORDER = (4, 3, 5, 2, 6, 1, 7)
NEAR_FIRST = (1, 7, 2, 6, 3, 5, 4)


class Phases:
    def __init__(self):
        self.open = None

    def __call__(self, name):
        if self.open is not None:
            self.open.__exit__(None, None, None)
        self.open = None
        if name is not None:
            self.open = jax.named_scope(name)
            self.open.__enter__()


def sigmoid(x):
    return jax.nn.sigmoid(x)


def dot_t(a, b):
    return lax.dot_general(a, b, (((0,), (0,)), ((), ())), preferred_element_type=F32)


def added(terms):
    return functools.reduce(lambda a, b: a + b, terms)


def kernel(
    scale, v_hbm, g_hbm, cot_hbm, w_hbm, gain_hbm, shift_hbm, ow_hbm,
    gv_out, gg_out, gw_out, sm_out,
    v_ref, g_ref, cot_ref, w_ref, gain_ref, shift_ref, ow_ref, gv_ref, gg_ref, gw_ref, lines,
    hv, hg, gated, normed, invs, dsil, ga, gcr, act, actp, cotp, wfull,
    far_st, opp_st, near_st, far_in, opp_in, near_in, near_own, gsum, spread_st, spread_in,
    t_a, t_b, rt_a, rt_b, fin_a, fin_b,
    taps, acc_gs, sm_all, sm_in, sm_ya, sm_zb, sm_za, sm_yb, sm_fin,
    send_sems, recv_sems, local_sems,
):
    phase = Phases()
    phase("start")
    rows, channels = v_ref.shape
    n_taps = w_ref.shape[0]
    blocks = channels // LANES
    features = ow_ref.shape[0]
    sp = lax.axis_index("sp")
    dp = lax.axis_index("dp")
    n_sp, n_dp = SIDE * SIDE, 2 * CHIPS
    z, y = sp // SIDE, sp % SIDE
    x, core = dp // 2, dp % 2
    step_x = 1 - 2 * core
    ahead_x = (x + CHIPS + step_x) % CHIPS
    behind_x = (x + CHIPS - step_x) % CHIPS
    far_x = (x + 2) % CHIPS

    other = {"sp": sp, "dp": 2 * x + (1 - core)}
    after = {"sp": (sp + 1) % n_sp, "dp": dp}
    before = {"sp": (sp + n_sp - 1) % n_sp, "dp": dp}
    at_y = {k: {"sp": z * SIDE + (y + k) % SIDE, "dp": dp} for k in range(1, SIDE)}
    at_z = {k: {"sp": ((z + k) % SIDE) * SIDE + y, "dp": dp} for k in range(1, SIDE)}
    at_dp = {k: {"sp": sp, "dp": (dp + k) % n_dp} for k in range(1, n_dp)}

    def chip(where):
        return {"sp": sp, "dp": 2 * where + core}

    barrier = pltpu.get_barrier_semaphore()
    peers = [after, before, *at_dp.values(), *at_y.values(), *at_z.values()]
    for peer in peers:
        pl.semaphore_signal(barrier, inc=1, device_id=peer, device_id_type=MESH)

    counter = [0, 0]
    started = []

    def remote(src, dst, device, i):
        return pltpu.make_async_remote_copy(
            src_ref=src, dst_ref=dst, send_sem=send_sems.at[i], recv_sem=recv_sems.at[i],
            device_id=device, device_id_type=MESH,
        )

    def send(src, dst, device):
        copy = remote(src, dst, device, counter[0])
        counter[0] += 1
        copy.start()
        started.append(copy)
        return copy

    def local(src, dst):
        copy = pltpu.make_async_copy(src, dst, local_sems.at[counter[1]])
        counter[1] += 1
        copy.start()
        return copy

    loads = [
        local(v_hbm, v_ref), local(g_hbm, g_ref), local(ow_hbm, ow_ref), local(cot_hbm, cot_ref),
        local(w_hbm, w_ref), local(gain_hbm, gain_ref), local(shift_hbm, shift_ref),
    ]

    def lanes(cb):
        return slice(cb * LANES, (cb + 1) * LANES)

    def gate_tile(i, _):
        base = pl.multiple_of(i * TILE, TILE)
        for cb in range(blocks):
            v = v_ref[pl.ds(base, TILE), lanes(cb)].astype(F32)
            g = g_ref[pl.ds(base, TILE), lanes(cb)].astype(F32)
            gated[cb, pl.ds(base + HALO, TILE), :] = v * sigmoid(g)
        return 0

    phase("loads")
    loads[0].wait()
    loads[1].wait()
    phase("gate")
    lax.fori_loop(0, rows // TILE, gate_tile, 0)
    phase("loads2")
    for copy in loads[2:]:
        copy.wait()
    phase("barrier")
    pl.semaphore_wait(barrier, len(peers))
    phase("issue")

    halo_v = send(v_ref.at[pl.ds(rows - HALO, HALO), :], hv, after)
    halo_g = send(g_ref.at[pl.ds(rows - HALO, HALO), :], hg, after)

    def columns(owner_x, owner_core):
        return pl.ds(pl.multiple_of((2 * owner_x + owner_core) * features, features), features)

    def shard(owner_x, owner_core):
        return wfull.at[columns(owner_x, owner_core), :]

    to_ahead = send(ow_ref, shard(x, core), chip(ahead_x))
    to_behind = send(ow_ref, shard(x, core), chip(behind_x))
    to_other = send(ow_ref, shard(x, core), other)
    cot_copies = [
        send(cot_ref.at[:, columns(k, 1 - core)], cotp.at[k], other) for k in range(CHIPS)
    ]
    wfull[columns(x, core), :] = ow_ref[...]

    def forward_step(i, _):
        base = pl.multiple_of(i * TILE, TILE)
        conv = []
        for cb in range(blocks):
            acc = jnp.zeros((TILE, LANES), F32)
            for j in range(n_taps):
                tap = w_ref[j : j + 1, lanes(cb)]
                acc = acc + tap * gated[cb, pl.ds(base + (j + HALO - n_taps + 1), TILE), :]
            conv.append(acc)
        mean = jnp.sum(added(conv), axis=-1, keepdims=True) * (1.0 / channels)
        centred = [c - mean for c in conv]
        var = jnp.sum(added([c * c for c in centred]), axis=-1, keepdims=True) * (1.0 / channels)
        inv = lax.rsqrt(var + EPS)
        invs[pl.ds(base, TILE), :] = jnp.broadcast_to(inv, (TILE, LANES))
        for cb in range(blocks):
            nrm = centred[cb] * inv
            pre = nrm * gain_ref[0:1, lanes(cb)] + shift_ref[0:1, lanes(cb)]
            sig = sigmoid(pre)
            normed[cb, pl.ds(base, TILE), :] = nrm
            act[pl.ds(base, TILE), lanes(cb)] = (pre * sig).astype(BF16)
            dsil[cb, pl.ds(base, TILE), :] = sig * (1.0 + pre * (1.0 - sig))
        return 0

    phase("forward")
    lax.fori_loop(1, rows // TILE, forward_step, 0)
    phase("halo_wait")
    halo_v.wait_recv()
    halo_g.wait_recv()
    phase("forward0")
    inside = (sp > 0).astype(F32)
    for cb in range(blocks):
        v = hv[:, lanes(cb)].astype(F32)
        g = hg[:, lanes(cb)].astype(F32)
        gated[cb, pl.ds(0, HALO), :] = v * sigmoid(g) * inside
    lax.fori_loop(0, 1, forward_step, 0)
    act_copy = send(act, actp, other)

    phase("act_wait")
    for copy in cot_copies:
        copy.wait_recv()
    act_copy.wait_recv()
    phase("product")
    pieces = (0, 2, 1, 3)

    def product(owner_x):
        cols = columns(owner_x, core)
        return dot_t(cot_ref[:, cols], act[...]) + dot_t(cotp[owner_x], actp[...])

    value = product(far_x).astype(BF16)
    for p in range(blocks):
        far_st[p] = value[:, lanes(p)]
    far_copies = {p: send(far_st.at[p], far_in.at[p], chip(ahead_x)) for p in pieces}
    value = product(behind_x).astype(BF16)
    for p in range(blocks):
        opp_st[p] = value[:, lanes(p)]
    opp_copies = {p: send(opp_st.at[p], opp_in.at[p], chip(behind_x)) for p in pieces}
    near_own[...] = product(ahead_x)
    gsum[...] = product(x)

    phase("w_wait1")
    to_ahead.wait_recv()
    to_behind.wait_recv()
    pass_far = send(shard(behind_x, core), shard(behind_x, core), chip(ahead_x))
    pass_1 = send(shard(behind_x, core), shard(behind_x, core), other)
    pass_2 = send(shard(ahead_x, core), shard(ahead_x, core), other)

    near_copies = {}

    def relay(p):
        far_copies[p].wait_recv()
        near_st[p] = (near_own[:, lanes(p)] + far_in[p].astype(F32)).astype(BF16)
        near_copies[p] = send(near_st.at[p], near_in.at[p], chip(ahead_x))

    phase("relay1")
    relay(0)
    relay(2)
    phase("w_wait2")
    pass_far.wait_recv()
    far_other = send(shard(far_x, core), shard(far_x, core), other)
    phase("relay2")
    relay(1)
    relay(3)
    phase("w_wait3")
    to_other.wait_recv()
    pass_1.wait_recv()
    pass_2.wait_recv()
    far_other.wait_recv()

    phase("matmul")
    half = rows // 2

    def matmul_step(i, _):
        base = pl.multiple_of(i * half, half)
        ga[pl.ds(base, half), :] = jnp.dot(
            cot_ref[pl.ds(base, half), :], wfull[...], preferred_element_type=F32
        )
        return 0

    lax.fori_loop(0, 2, matmul_step, 0)
    phase("grad")
    acc_gs[...] = jnp.zeros_like(acc_gs)
    taps[...] = jnp.zeros_like(taps)

    def fold(a):
        return a.reshape(TILE // 8, 8, LANES).sum(axis=0)

    def grad_step(i, _):
        base = pl.multiple_of(i * TILE, TILE)
        grads, norms = [], []
        for cb in range(blocks):
            gpre = ga[pl.ds(base, TILE), lanes(cb)] * dsil[cb, pl.ds(base, TILE), :]
            nrm = normed[cb, pl.ds(base, TILE), :]
            acc_gs[0, cb] = acc_gs[0, cb] + fold(gpre * nrm)
            acc_gs[1, cb] = acc_gs[1, cb] + fold(gpre)
            grads.append(gpre * gain_ref[0:1, lanes(cb)])
            norms.append(nrm)
        mean = jnp.sum(added(grads), axis=-1, keepdims=True) * (1.0 / channels)
        along = added([a * b for a, b in zip(grads, norms)])
        mean_along = jnp.sum(along, axis=-1, keepdims=True) * (1.0 / channels)
        inv = invs[pl.ds(base, TILE), :]
        for cb in range(blocks):
            gcr[cb, pl.ds(base, TILE), :] = inv * (grads[cb] - mean - norms[cb] * mean_along)
        return 0

    lax.fori_loop(0, 1, grad_step, 0)
    halo_c = send(gcr.at[:, pl.ds(0, HALO), :], gcr.at[:, pl.ds(rows, HALO), :], before)
    lax.fori_loop(1, rows // TILE, grad_step, 0)

    part = features // SIDE

    spread_copies = {}

    def chip_sum(p):
        near_copies[p].wait_recv()
        opp_copies[p].wait_recv()
        total = gsum[:, lanes(p)] + near_in[p].astype(F32) + opp_in[p].astype(F32)
        gsum[:, lanes(p)] = total
        spread_st[p] = total.astype(BF16)
        mine, at = (y, at_y) if p < 2 else (z, at_z)
        for k in ORDER:
            chunk = pl.ds(pl.multiple_of(((mine + k) % SIDE) * part, part), part)
            spread_copies[p, k] = send(spread_st.at[p, chunk, :], spread_in.at[p, k - 1], at[k])

    phase("chip_sum1")
    chip_sum(0)
    chip_sum(2)

    def taps_step(i, _):
        base = pl.multiple_of(i * TILE, TILE)
        for cb in range(blocks):
            own = gated[cb, pl.ds(base + HALO, TILE), :]
            for j in range(n_taps):
                shifted = gcr[cb, pl.ds(base + (n_taps - 1 - j), TILE), :]
                taps[cb, j] = taps[cb, j] + fold(own * shifted)
        return 0

    n_tiles = rows // TILE
    phase("taps1")
    lax.fori_loop(0, n_tiles // 2, taps_step, 0)
    phase("chip_sum2")
    chip_sum(1)
    chip_sum(3)
    phase("halo_c")
    halo_c.wait_recv()
    beyond = (sp < n_sp - 1).astype(F32)
    for cb in range(blocks):
        gcr[cb, pl.ds(rows, HALO), :] = gcr[cb, pl.ds(rows, HALO), :] * beyond
    phase("taps2")
    lax.fori_loop(n_tiles // 2, n_tiles, taps_step, 0)

    phase("small_fold")
    per_block = SMALL // 8
    row_ids = lax.broadcasted_iota(jnp.int32, (8, LANES), 0)
    for t in range(n_dp * OWN_TILES):
        cb, rb = t // per_block, t % per_block
        tile = jnp.zeros((8, LANES), F32)
        if cb < blocks:
            for r in range(8):
                j = rb * 8 + r
                if j < n_taps:
                    line = taps[cb, j]
                elif j < n_taps + 2:
                    line = acc_gs[j - n_taps, cb]
                else:
                    continue
                line = jnp.sum(line, axis=0, keepdims=True) * scale
                tile = jnp.where(row_ids == r, line, tile)
        sm_all[t // OWN_TILES, t % OWN_TILES] = tile
    small_rs = [send(sm_all.at[(dp + k) % n_dp], sm_in.at[k - 1], at_dp[k]) for k in range(1, n_dp)]

    def backward_step(i, _):
        base = pl.multiple_of(i * TILE, TILE)
        for cb in range(blocks):
            acc = jnp.zeros((TILE, LANES), F32)
            for j in range(n_taps):
                tap = w_ref[j : j + 1, lanes(cb)]
                acc = acc + tap * gcr[cb, pl.ds(base + (n_taps - 1 - j), TILE), :]
            v = v_ref[pl.ds(base, TILE), lanes(cb)].astype(F32)
            sig = sigmoid(g_ref[pl.ds(base, TILE), lanes(cb)].astype(F32))
            gs = acc * sig
            gv_ref[pl.ds(base, TILE), lanes(cb)] = gs.astype(BF16)
            gg_ref[pl.ds(base, TILE), lanes(cb)] = (gs * v * (1.0 - sig)).astype(BF16)
        return 0

    phase("rs1_wait")
    for copy in spread_copies.values():
        copy.wait_recv()
    phase("rs1_sum")

    def first_sum(own_index, first_piece, t_ref):
        chunk = pl.ds(pl.multiple_of(own_index * part, part), part)
        for c in range(2):
            p = first_piece + c
            total = gsum[chunk, lanes(p)]
            for k in range(SIDE - 1):
                total = total + spread_in[p, k].astype(F32)
            total = total * scale
            for r in range(part // 8):
                t_ref[2 * r + c] = total[r * 8 : r * 8 + 8, :]

    first_sum(y, 0, t_a)
    first_sum(z, 2, t_b)
    second_a, second_b = [], []
    for k in ORDER:
        second_a.append(send(t_a.at[(z + k) % SIDE], rt_a.at[k - 1], at_z[k]))
        second_b.append(send(t_b.at[(y + k) % SIDE], rt_b.at[k - 1], at_y[k]))

    phase("backward1")
    lax.fori_loop(0, n_tiles // 2, backward_step, 0)

    phase("small_rs")
    for copy in small_rs:
        copy.wait_recv()
    total = sm_all[dp]
    for k in range(n_dp - 1):
        total = total + sm_in[k]
    sm_ya[y] = total[:2]
    sm_zb[z] = total[2:]
    small_1 = []
    for k in ORDER:
        small_1.append(send(sm_ya.at[y], sm_ya.at[y], at_y[k]))
        small_1.append(send(sm_zb.at[z], sm_zb.at[z], at_z[k]))

    phase("rs2_wait")
    for copy in second_a + second_b:
        copy.wait_recv()
    fin_a[y, z] = t_a[z] + added([rt_a[k] for k in range(SIDE - 1)])
    fin_b[z, y] = t_b[y] + added([rt_b[k] for k in range(SIDE - 1)])
    phase("ag1_issue")
    along_a = {k: send(fin_a.at[y, z], fin_a.at[y, z], at_z[k]) for k in ORDER}
    along_b = {k: send(fin_b.at[z, y], fin_b.at[z, y], at_y[k]) for k in ORDER}

    across = {k: counter[0] + k - 1 for k in range(1, SIDE)}
    counter[0] += 2 * (SIDE - 1)

    def pass_on(a_z, b_y):
        for k in ORDER:
            tile = fin_a.at[y, a_z]
            remote(tile, tile, at_y[k], across[k]).start()
            tile = fin_b.at[z, b_y]
            remote(tile, tile, at_z[k], across[k] + SIDE - 1).start()

    pass_on(z, y)
    phase("backward2")
    lax.fori_loop(n_tiles // 2, n_tiles, backward_step, 0)
    stores = [local(gv_ref, gv_out), local(gg_ref, gg_out)]

    phase("small_1")
    for copy in small_1:
        copy.wait_recv()
    sm_za[z] = added([sm_ya[k] for k in range(SIDE)])
    sm_yb[y] = added([sm_zb[k] for k in range(SIDE)])
    small_2 = []
    for k in ORDER:
        small_2.append(send(sm_za.at[z], sm_za.at[z], at_z[k]))
        small_2.append(send(sm_yb.at[y], sm_yb.at[y], at_y[k]))

    phase("ag_pass")
    for k in NEAR_FIRST:
        along_a[k].wait_recv()
        along_b[k].wait_recv()
        pass_on((z + SIDE - k) % SIDE, (y + SIDE - k) % SIDE)

    phase("small_2")
    for copy in small_2:
        copy.wait_recv()
    sm_fin[dp, :2] = added([sm_za[k] for k in range(SIDE)])
    sm_fin[dp, 2:] = added([sm_yb[k] for k in range(SIDE)])
    small_ag = [send(sm_fin.at[dp], sm_fin.at[dp], at_dp[k]) for k in range(1, n_dp)]

    phase("ag2_wait")
    groups = []
    for k in range(1, SIDE):
        groups.append(remote(fin_a.at[y], fin_a.at[y], at_y[k], across[k]))
        groups.append(remote(fin_b.at[z], fin_b.at[z], at_z[k], across[k] + SIDE - 1))
    for group in groups:
        group.wait_recv()
    phase("assemble")
    width = channels // 2
    for r in range(SIDE):
        for t in range(SIDE):
            line = slice(r * part + (t // 2) * 8, r * part + (t // 2) * 8 + 8)
            c = (t % 2) * LANES
            gw_ref[line, c : c + LANES] = fin_a[r, t]
            gw_ref[line, width + c : width + c + LANES] = fin_b[r, t]
    stores.append(local(gw_ref, gw_out))

    phase("small_ag")
    for copy in small_ag:
        copy.wait_recv()
    for t in range(blocks * per_block):
        cb, rb = t // per_block, t % per_block
        lines[rb * 8 : rb * 8 + 8, lanes(cb)] = sm_fin[t // OWN_TILES, t % OWN_TILES]
    stores.append(local(lines, sm_out))
    phase("send_wait")
    for copy in started:
        copy.wait_send()
    for group in groups:
        group.wait_send()
    for copy in stores:
        copy.wait()
    phase(None)


def hand_out(gv, gg, gw, lines, gv_out, gg_out, gw_out, taps, gain, shift):
    n_taps = taps.shape[0]
    gv_out[...] = gv[...]
    gg_out[...] = gg[...]
    gw_out[...] = gw[...]
    taps[...] = lines[:n_taps]
    gain[...] = lines[n_taps : n_taps + 1]
    shift[...] = lines[n_taps + 1 : n_taps + 2]


def per_device(count, glu_value, glu_gate, cotangent, conv_weight, norm_gain, norm_shift, out_weight):
    value, gate, cot = glu_value[0], glu_gate[0], cotangent[0]
    rows, channels = value.shape
    n_taps = conv_weight.shape[0]
    features = out_weight.shape[0]
    blocks = channels // LANES
    part = features // SIDE
    n_dp = 2 * CHIPS
    scale = 1.0 / math.sqrt(rows * count)
    hbm = pl.BlockSpec(memory_space=pltpu.HBM)
    anywhere = pl.BlockSpec(memory_space=pl.ANY)
    vmem = pl.BlockSpec(memory_space=pltpu.VMEM)
    shape = jax.ShapeDtypeStruct
    buffer = pltpu.VMEM
    tile = (8, LANES)
    piece = (blocks, features, LANES)
    outs = pl.pallas_call(
        functools.partial(kernel, scale),
        out_shape=[
            pltpu.VMEM((rows, channels), BF16),
            pltpu.VMEM((rows, channels), BF16),
            pltpu.VMEM((features, channels), F32),
            pltpu.VMEM((SMALL, channels), F32),
        ],
        in_specs=[hbm] * 7,
        out_specs=[anywhere] * 4,
        scratch_shapes=[
            buffer((rows, channels), BF16),
            buffer((rows, channels), BF16),
            buffer(cot.shape, BF16),
            buffer((n_taps, channels), F32),
            buffer((1, channels), F32),
            buffer((1, channels), F32),
            buffer((features, channels), BF16),
            buffer((rows, channels), BF16),
            buffer((rows, channels), BF16),
            buffer((features, channels), F32),
            buffer((SMALL, channels), F32),
            buffer((HALO, channels), BF16),
            buffer((HALO, channels), BF16),
            buffer((blocks, rows + HALO, LANES), F32),
            buffer((blocks, rows, LANES), F32),
            buffer((rows, LANES), F32),
            buffer((blocks, rows, LANES), F32),
            buffer((rows, channels), F32),
            buffer((blocks, rows + HALO, LANES), F32),
            buffer((rows, channels), BF16),
            buffer((rows, channels), BF16),
            buffer((CHIPS, rows, features), BF16),
            buffer((n_dp * features, channels), BF16),
            buffer(piece, BF16),
            buffer(piece, BF16),
            buffer(piece, BF16),
            buffer(piece, BF16),
            buffer(piece, BF16),
            buffer(piece, BF16),
            buffer((features, channels), F32),
            buffer((features, channels), F32),
            buffer(piece, BF16),
            buffer((blocks, SIDE - 1, part, LANES), BF16),
            buffer((SIDE, *tile), F32),
            buffer((SIDE, *tile), F32),
            buffer((SIDE - 1, *tile), F32),
            buffer((SIDE - 1, *tile), F32),
            buffer((SIDE, SIDE, *tile), F32),
            buffer((SIDE, SIDE, *tile), F32),
            buffer((blocks, n_taps, *tile), F32),
            buffer((2, blocks, *tile), F32),
            buffer((n_dp, OWN_TILES, *tile), F32),
            buffer((n_dp - 1, OWN_TILES, *tile), F32),
            buffer((SIDE, 2, *tile), F32),
            buffer((SIDE, OWN_TILES - 2, *tile), F32),
            buffer((SIDE, 2, *tile), F32),
            buffer((SIDE, OWN_TILES - 2, *tile), F32),
            buffer((n_dp, OWN_TILES, *tile), F32),
            pltpu.SemaphoreType.DMA((COPIES,)),
            pltpu.SemaphoreType.DMA((COPIES,)),
            pltpu.SemaphoreType.DMA((16,)),
        ],
        compiler_params=pltpu.CompilerParams(
            collective_id=0, has_side_effects=True, vmem_limit_bytes=62 * 2**20
        ),
        name="backward",
    )(value, gate, cot, conv_weight, norm_gain[None], norm_shift[None], out_weight)
    grad_value, grad_gate, grad_weight, grad_taps, grad_gain, grad_shift = pl.pallas_call(
        hand_out,
        out_shape=[
            shape((rows, channels), BF16),
            shape((rows, channels), BF16),
            shape((features, channels), F32),
            shape((n_taps, channels), F32),
            shape((1, channels), F32),
            shape((1, channels), F32),
        ],
        in_specs=[vmem] * 4,
        out_specs=[vmem] * 6,
        compiler_params=pltpu.CompilerParams(vmem_limit_bytes=16 * 2**20),
        name="hand_out",
    )(*outs)
    return (
        grad_value[None], grad_gate[None], grad_weight,
        grad_taps, grad_gain.reshape(channels), grad_shift.reshape(channels),
    )


def solution(mesh):
    return jax.shard_map(
        functools.partial(per_device, mesh.size),
        mesh=mesh,
        in_specs=(
            P("dp", "sp", None), P("dp", "sp", None), P("dp", "sp", None),
            P(), P(), P(), P("dp", None),
        ),
        out_specs=(P("dp", "sp", None), P("dp", "sp", None), P("dp", None), P(), P(), P()),
        check_vma=False,
    )
```

time: 82.4 us -> 65.4 us (0.79)
  Pallas kernels: 74.1 us -> 64.6 us
  local copies, waits for them, and re-layouts: 7.38 us -> 0 us
    pallas_call x1 -> x2, Pallas kernels: 74.1 us -> 64.6 us  [the longest x1 63.3 us: per_device(): pl.pallas_call(functools.partial(kernel, scale), out_shape=[pltpu.VMEM((r...]
    unnamed x5 -> x0, local copies, waits for them, and re-layouts: 4.53 us -> none
    slice x2 -> x0, local copies, waits for them, and re-layouts: 2.85 us -> none  [the longest x1 1.47 us: per_device(): lines[:n_taps]]
where the time goes in v2:
time: 65.4 us; the launch traced here: 65.2 us
  Pallas kernels  64.6 us (99%)
    pallas_call x1, Pallas kernels, per_device(): pl.pallas_call(functools.partial(kernel, scale), out_shape=[pltpu.VMEM((r...  63.3 us

profile of v2, /device:TPU:1, one launch (start us, length us, event | category | flops | bytes accessed | tf_op | source)
XLA Modules:
  0.0 65.2 jit_solution(824117312244717864)
XLA Ops:
  0.6 63.3 %backward.1 = (bf16[512,512]{1,0:T(8,128)(2,1)S(1)}, bf16[512,512]{1,0:T(8,128)(2,1)S(1)}, f32[256,512]{1,0:T(8,128)S(1)}, f32[40,512]{1,0:T(8,128)S(1)}) custom-call(bf16[512,512]{1,0:T(8,128)(2,1)} %bitcast.10, bf16[512,512]{1,0:T(8,128)(2,1)} %bitcast.11, bf16[512,2048]{1,0:T(8,128)(2,1)} %bitcast.9, f32[31,512]{1,0:T(8,128)} %w_hbm.1, ...), custom_call_target="tpu_custom_call" | custom-call | tf_op jit(solution)/shard_map/backward/pallas_call | solution.py:511
  63.9 1.3 %hand_out.1 = (bf16[512,512]{1,0:T(8,128)(2,1)}, bf16[512,512]{1,0:T(8,128)(2,1)}, f32[256,512]{1,0:T(8,128)}, f32[31,512]{1,0:T(8,128)}, f32[1,512]{1,0:T(1,128)}, /*index=5*/f32[1,512]{1,0:T(1,128)}) custom-call(bf16[512,512]{1,0:T(8,128)(2,1)S(1)} %get-tuple-element.16.gv, bf16[512,512]{1,0:T(8,128)(2,1)S(1)} %get-tuple-element.17.gg, ...), custom_call_target="tpu_custom_call" | custom-call | tf_op jit(solution)/shard_map/hand_out/pallas_call | solution.py:579

commit v3 on v2

v3 whole, which is shorter than its diff:
```python
import functools
import math

import jax
import jax.numpy as jnp
from jax import lax
from jax.experimental import pallas as pl
from jax.experimental.pallas import tpu as pltpu
from jax.sharding import PartitionSpec as P

MESH = pl.DeviceIdType.MESH
F32 = jnp.float32
BF16 = jnp.bfloat16

EPS = 1e-06
LANES = 128
HALO = 32
TILE = 64
SIDE = 8
CHIPS = 4
RECEIVE_SEMS = 45
SEND_SEMS = 19
SMALL = 40
OWN_TILES = 3
ORDER = (4, 3, 5, 2, 6, 1, 7)
NEAR_FIRST = (1, 7, 2, 6, 3, 5, 4)


class Phases:
    def __init__(self):
        self.open = None

    def __call__(self, name):
        if self.open is not None:
            self.open.__exit__(None, None, None)
        self.open = None
        if name is not None:
            self.open = jax.named_scope(name)
            self.open.__enter__()


def sigmoid(x):
    return jax.nn.sigmoid(x)


def dot_t(a, b):
    return lax.dot_general(a, b, (((0,), (0,)), ((), ())), preferred_element_type=F32)


def added(terms):
    return functools.reduce(lambda a, b: a + b, terms)


def kernel(
    scale, v_hbm, g_hbm, cot_hbm, w_hbm, gain_hbm, shift_hbm, ow_hbm,
    gv_ref, gg_ref, gw_ref, taps_ref, grad_gain, grad_shift,
    v_ref, g_ref, cot_ref, w_ref, gain_ref, shift_ref, ow_ref,
    halo, halo_next, gated, normed, invs, dsil, ga, gcr, act, actp, cotp, wfull,
    far_st, opp_st, near_st, far_in, opp_in, near_in, near_own, own_part, gsum, cross_st, cross_own, cross_in, cross_sum, cross_x, spread_st, spread_in,
    t_a, t_b, rt_a, rt_b, fin_a, fin_b,
    taps, acc_gs, sm_all, sm_in, sm_ya, sm_zb, sm_za, sm_yb, sm_fin,
    send_sems, recv_sems, local_sems,
):
    phase = Phases()
    phase("start")
    rows, channels = v_ref.shape
    n_taps = w_ref.shape[0]
    blocks = channels // LANES
    features = ow_ref.shape[0]
    sp = lax.axis_index("sp")
    dp = lax.axis_index("dp")
    n_sp, n_dp = SIDE * SIDE, 2 * CHIPS
    z, y = sp // SIDE, sp % SIDE
    x, core = dp // 2, dp % 2
    step_x = 1 - 2 * core
    ahead_x = (x + CHIPS + step_x) % CHIPS
    behind_x = (x + CHIPS - step_x) % CHIPS
    far_x = (x + 2) % CHIPS

    other = {"sp": sp, "dp": 2 * x + (1 - core)}
    after = {"sp": (sp + 1) % n_sp, "dp": dp}
    before = {"sp": (sp + n_sp - 1) % n_sp, "dp": dp}
    at_y = {k: {"sp": z * SIDE + (y + k) % SIDE, "dp": dp} for k in range(1, SIDE)}
    at_z = {k: {"sp": ((z + k) % SIDE) * SIDE + y, "dp": dp} for k in range(1, SIDE)}
    at_dp = {k: {"sp": sp, "dp": (dp + k) % n_dp} for k in range(1, n_dp)}

    def chip(where):
        return {"sp": sp, "dp": 2 * where + core}

    barrier = pltpu.get_barrier_semaphore()
    peers = [after, before, *at_dp.values(), *at_y.values(), *at_z.values()]
    for peer in peers:
        pl.semaphore_signal(barrier, inc=1, device_id=peer, device_id_type=MESH)

    receive_ids, send_ids = {}, {}

    def remote(src, dst, device, got, sent):
        return pltpu.make_async_remote_copy(
            src_ref=src, dst_ref=dst,
            send_sem=send_sems.at[send_ids.setdefault(sent, len(send_ids))],
            recv_sem=recv_sems.at[receive_ids.setdefault(got, len(receive_ids))],
            device_id=device, device_id_type=MESH,
        )

    def send(src, dst, device, got, sent):
        remote(src, dst, device, got, sent).start()

    def arrived(got, size):
        remote(size, size, other, got, "w").wait_recv()

    def left(sent, size):
        remote(size, size, other, "pair_w", sent).wait_send()

    counter = [0]

    def local(src, dst):
        copy = pltpu.make_async_copy(src, dst, local_sems.at[counter[0]])
        counter[0] += 1
        copy.start()
        return copy

    loads = [
        local(v_hbm, v_ref), local(g_hbm, g_ref), local(ow_hbm, ow_ref), local(cot_hbm, cot_ref.at[pl.ds(0, rows), :]),
        local(w_hbm, w_ref), local(gain_hbm, gain_ref), local(shift_hbm, shift_ref),
    ]

    def lanes(cb):
        return slice(cb * LANES, (cb + 1) * LANES)

    def gate_tile(i, _):
        base = pl.multiple_of(i * TILE, TILE)
        for cb in range(blocks):
            v = v_ref[pl.ds(base, TILE), lanes(cb)].astype(F32)
            g = g_ref[pl.ds(base, TILE), lanes(cb)].astype(F32)
            gated[cb, pl.ds(base + HALO, TILE), :] = v * sigmoid(g)
        return 0

    phase("loads")
    loads[0].wait()
    loads[1].wait()
    phase("gate")
    lax.fori_loop(0, rows // TILE, gate_tile, 0)
    phase("loads2")
    for copy in loads[2:]:
        copy.wait()
    phase("barrier")
    pl.semaphore_wait(barrier, len(peers))
    phase("issue")

    send(v_ref.at[pl.ds(rows - HALO, HALO), :], halo.at[0], after, "halo", "halo")
    send(g_ref.at[pl.ds(rows - HALO, HALO), :], halo.at[1], after, "halo", "halo")
    send(v_ref.at[pl.ds(0, HALO), :], halo_next.at[0], before, "next", "next")
    send(g_ref.at[pl.ds(0, HALO), :], halo_next.at[1], before, "next", "next")
    next_rows = cot_ref.at[pl.ds(rows, HALO), :]

    def columns(owner_x, owner_core):
        return pl.ds(pl.multiple_of((2 * owner_x + owner_core) * features, features), features)

    def shard(owner_x, owner_core):
        return wfull.at[columns(owner_x, owner_core), :]

    parity = (y + z) % 2
    half_rows, quarter_rows = features // 2, features // 8

    def shard_half(owner_x, which):
        first = (2 * owner_x + core) * features + which * half_rows
        return wfull.at[pl.ds(pl.multiple_of(first, half_rows), half_rows), :]

    def shard_quarter(owner_x, i):
        first = (2 * owner_x + core) * features + parity * half_rows + i * quarter_rows
        return wfull.at[pl.ds(pl.multiple_of(first, quarter_rows), quarter_rows), :]

    own_half = ow_ref.at[pl.ds(pl.multiple_of(parity * half_rows, half_rows), half_rows), :]
    send(own_half, shard_half(x, parity), chip(ahead_x), "ahead", "w")
    send(own_half, shard_half(x, parity), chip(behind_x), "behind", "w")
    send(ow_ref, shard(x, core), other, "pair_w", "w")
    around = (at_y[1], at_y[SIDE - 1], at_z[1], at_z[SIDE - 1])

    def pass_half(owner_x, name):
        half_in = shard_half(owner_x, parity)
        for i in range(4):
            quarter = shard_quarter(owner_x, i)
            send(quarter, quarter, around[i], name, "w")
        send(half_in, half_in, other, "pair_w", "w")

    def pass_rest(owner_x, name):
        rest = shard_half(owner_x, 1 - parity)
        arrived(name, rest)
        send(rest, rest, other, "pair_w", "w")

    for k in range(CHIPS):
        send(cot_ref.at[pl.ds(0, rows), columns(k, 1 - core)], cotp.at[k], other, "cot", "cot")
    wfull[columns(x, core), :] = ow_ref[...]

    def conv_rows(base, size):
        for cb in range(blocks):
            acc = jnp.zeros((size, LANES), F32)
            for j in range(n_taps):
                tap = w_ref[j : j + 1, lanes(cb)]
                acc = acc + tap * gated[cb, pl.ds(base + (j + HALO - n_taps + 1), size), :]
            normed[cb, pl.ds(base, size), :] = acc

    def norm_rows(base, size, own=True):
        conv = [normed[cb, pl.ds(base, size), :] for cb in range(blocks)]
        mean = jnp.sum(added(conv), axis=-1, keepdims=True) * (1.0 / channels)
        centred = [c - mean for c in conv]
        var = jnp.sum(added([c * c for c in centred]), axis=-1, keepdims=True) * (1.0 / channels)
        inv = lax.rsqrt(var + EPS)
        invs[pl.ds(base, size), :] = jnp.broadcast_to(inv, (size, LANES))
        for cb in range(blocks):
            nrm = centred[cb] * inv
            pre = nrm * gain_ref[0:1, lanes(cb)] + shift_ref[0:1, lanes(cb)]
            sig = sigmoid(pre)
            normed[cb, pl.ds(base, size), :] = nrm
            if own:
                act[pl.ds(base, size), lanes(cb)] = (pre * sig).astype(BF16)
            dsil[cb, pl.ds(base, size), :] = sig * (1.0 + pre * (1.0 - sig))

    def over_tiles(first_tile, last_tile, step):
        def body(i, _):
            step(pl.multiple_of(i * TILE, TILE), TILE)
            return 0

        lax.fori_loop(first_tile, last_tile, body, 0)

    def forward(first_tile, last_tile):
        over_tiles(first_tile, last_tile, conv_rows)
        over_tiles(first_tile, last_tile, norm_rows)

    def send_act(first, last):
        lines = pl.ds(first * TILE, (last - first) * TILE)
        send(act.at[lines, :], actp.at[lines, :], other, "act", "act")

    n_tiles = rows // TILE
    phase("forward")
    forward(1, n_tiles // 2)
    send_act(1, n_tiles // 2)
    forward(n_tiles // 2, n_tiles)
    send_act(n_tiles // 2, n_tiles)
    phase("halo_wait")
    arrived("halo", halo)
    phase("forward0")
    inside = (sp > 0).astype(F32)
    for cb in range(blocks):
        v = halo[0, :, lanes(cb)].astype(F32)
        g = halo[1, :, lanes(cb)].astype(F32)
        gated[cb, pl.ds(0, HALO), :] = v * sigmoid(g) * inside
    forward(0, 1)
    send_act(0, 1)

    phase("w_wait1")
    arrived("ahead", shard_half(behind_x, parity))
    passed = shard_half(behind_x, parity)
    send(passed, passed, chip(ahead_x), "far", "w")
    pass_half(behind_x, "quarters_behind")
    arrived("behind", shard_half(ahead_x, parity))
    pass_half(ahead_x, "quarters_ahead")
    send(cot_ref.at[pl.ds(0, HALO), :], next_rows, before, "next_cot", "next_cot")

    phase("forward_next")
    arrived("next", halo_next)
    for cb in range(blocks):
        v = halo_next[0, :, lanes(cb)].astype(F32)
        g = halo_next[1, :, lanes(cb)].astype(F32)
        gated[cb, pl.ds(rows + HALO, HALO), :] = v * sigmoid(g)
    conv_rows(rows, HALO)
    norm_rows(rows, HALO, own=False)

    pieces, crossing = (0, 1), (2, 3)
    part = features // SIDE
    mine, around_all = (y, z, y, z), (at_y, at_z, at_y, at_z)

    def chunk_of(where):
        return pl.ds(pl.multiple_of(where * part, part), part)

    def own_product(owner_x):
        return dot_t(cot_ref[pl.ds(0, rows), columns(owner_x, core)], act[...])

    def other_product(owner_x):
        return dot_t(cotp[owner_x], actp[...])

    phase("product0")
    own_part[0] = own_product(far_x)
    own_part[1] = own_product(behind_x)
    phase("act_wait")
    arrived("cot", cotp)
    arrived("act", actp)
    phase("product")
    def kept(owner_x, value, store):
        rounded = value.astype(BF16)
        for p in crossing:
            cross_own[p - 2, owner_x] = value[:, lanes(p)]
            cross_st[p - 2, owner_x] = rounded[:, lanes(p)]
        for p in pieces:
            store[p] = (value if store.dtype == F32 else rounded)[:, lanes(p)]

    kept(far_x, own_part[0] + other_product(far_x), far_st)
    for p in pieces:
        send(far_st.at[p], far_in.at[p], chip(ahead_x), ("far", p), "far")
    kept(behind_x, own_part[1] + other_product(behind_x), opp_st)
    for p in pieces:
        send(opp_st.at[p], opp_in.at[p], chip(behind_x), ("opp", p), "opp")
    kept(ahead_x, own_product(ahead_x) + other_product(ahead_x), near_own)
    kept(x, own_product(x) + other_product(x), gsum)
    def relay(p):
        arrived(("far", p), far_in.at[p])
        near_st[p] = (near_own[p] + far_in[p].astype(F32)).astype(BF16)
        send(near_st.at[p], near_in.at[p], chip(ahead_x), ("near", p), "near")

    phase("w_rest0")
    pass_rest(behind_x, "quarters_behind")
    passed_rest = shard_half(behind_x, 1 - parity)
    send(passed_rest, passed_rest, chip(ahead_x), "far_rest", "w")
    phase("w_rest1")
    pass_rest(ahead_x, "quarters_ahead")
    for k in ORDER:
        for p in crossing:
            source = cross_st.at[p - 2, :, chunk_of((mine[p] + k) % SIDE), :]
            send(source, cross_in.at[p - 2, k - 1], around_all[p][k], "cross", "cross")
    phase("w_wait2")
    for name, which in (("far", parity), ("far_rest", 1 - parity)):
        far_half = shard_half(far_x, which)
        arrived(name, far_half)
        send(far_half, far_half, other, "pair_w", "w")
    phase("relay0")
    relay(0)
    relay(1)
    phase("w_wait4")
    arrived("pair_w", wfull.at[pl.ds(0, CHIPS * features), :])

    phase("matmul")
    arrived("next_cot", next_rows)
    half = (rows + HALO) // 2

    def matmul_step(i, _):
        base = pl.multiple_of(i * half, 16)
        ga[pl.ds(base, half), :] = jnp.dot(
            cot_ref[pl.ds(base, half), :], wfull[...], preferred_element_type=F32
        )
        return 0

    lax.fori_loop(0, 2, matmul_step, 0)
    phase("grad")
    acc_gs[...] = jnp.zeros_like(acc_gs)
    taps[...] = jnp.zeros_like(taps)

    def fold(a):
        return a.reshape(TILE // 8, 8, LANES).sum(axis=0)

    def grad_rows(base, size, own=True):
        grads, norms = [], []
        for cb in range(blocks):
            gpre = ga[pl.ds(base, size), lanes(cb)] * dsil[cb, pl.ds(base, size), :]
            nrm = normed[cb, pl.ds(base, size), :]
            if own:
                acc_gs[0, cb] = acc_gs[0, cb] + fold(gpre * nrm)
                acc_gs[1, cb] = acc_gs[1, cb] + fold(gpre)
            grads.append(gpre * gain_ref[0:1, lanes(cb)])
            norms.append(nrm)
        mean = jnp.sum(added(grads), axis=-1, keepdims=True) * (1.0 / channels)
        along = added([a * b for a, b in zip(grads, norms)])
        mean_along = jnp.sum(along, axis=-1, keepdims=True) * (1.0 / channels)
        inv = invs[pl.ds(base, size), :]
        for cb in range(blocks):
            gcr[cb, pl.ds(base, size), :] = inv * (grads[cb] - mean - norms[cb] * mean_along)

    over_tiles(0, n_tiles, grad_rows)
    grad_rows(rows, HALO, own=False)
    beyond = (sp < n_sp - 1).astype(F32)
    for cb in range(blocks):
        gcr[cb, pl.ds(rows, HALO), :] = gcr[cb, pl.ds(rows, HALO), :] * beyond

    def chip_sum(p):
        arrived(("near", p), near_in.at[p])
        arrived(("opp", p), opp_in.at[p])
        total = gsum[p] + near_in[p].astype(F32) + opp_in[p].astype(F32)
        gsum[p] = total
        spread_st[p] = total.astype(BF16)
        for k in ORDER:
            source = spread_st.at[p, chunk_of((mine[p] + k) % SIDE), :]
            send(source, spread_in.at[p, k - 1], around_all[p][k], "spread", "spread")

    phase("chip_sum")
    for p in pieces:
        chip_sum(p)

    def taps_step(i, _):
        base = pl.multiple_of(i * TILE, TILE)
        for cb in range(blocks):
            own = gated[cb, pl.ds(base + HALO, TILE), :]
            for j in range(n_taps):
                shifted = gcr[cb, pl.ds(base + (n_taps - 1 - j), TILE), :]
                taps[cb, j] = taps[cb, j] + fold(own * shifted)
        return 0

    phase("taps1")
    lax.fori_loop(0, n_tiles // 2, taps_step, 0)
    phase("cross_wait")
    arrived("cross", cross_in)
    for p in crossing:
        for owner in range(CHIPS):
            total = cross_own[p - 2, owner, chunk_of(mine[p]), :]
            for k in range(SIDE - 1):
                total = total + cross_in[p - 2, k, owner].astype(F32)
            cross_sum[p - 2, owner] = total
        for k in (2, 1, 3):
            to = (x + k) % CHIPS
            send(cross_sum.at[p - 2, to], cross_x.at[p - 2, k - 1], chip(to), "cross_x", "cross_x")
    phase("taps2")
    lax.fori_loop(n_tiles // 2, n_tiles, taps_step, 0)

    phase("small_fold")
    per_block = SMALL // 8
    row_ids = lax.broadcasted_iota(jnp.int32, (8, LANES), 0)
    for t in range(n_dp * OWN_TILES):
        cb, rb = t // per_block, t % per_block
        tile = jnp.zeros((8, LANES), F32)
        if cb < blocks:
            for r in range(8):
                j = rb * 8 + r
                if j < n_taps:
                    line = taps[cb, j]
                elif j < n_taps + 2:
                    line = acc_gs[j - n_taps, cb]
                else:
                    continue
                line = jnp.sum(line, axis=0, keepdims=True) * scale
                tile = jnp.where(row_ids == r, line, tile)
        sm_all[t // OWN_TILES, t % OWN_TILES] = tile
    for k in range(1, n_dp):
        send(sm_all.at[(dp + k) % n_dp], sm_in.at[k - 1], at_dp[k], "small_0", "small_0")

    def backward_step(i, _):
        base = pl.multiple_of(i * TILE, TILE)
        for cb in range(blocks):
            acc = jnp.zeros((TILE, LANES), F32)
            for j in range(n_taps):
                tap = w_ref[j : j + 1, lanes(cb)]
                acc = acc + tap * gcr[cb, pl.ds(base + (n_taps - 1 - j), TILE), :]
            v = v_ref[pl.ds(base, TILE), lanes(cb)].astype(F32)
            sig = sigmoid(g_ref[pl.ds(base, TILE), lanes(cb)].astype(F32))
            gs = acc * sig
            gv_ref[pl.ds(base, TILE), lanes(cb)] = gs.astype(BF16)
            gg_ref[pl.ds(base, TILE), lanes(cb)] = (gs * v * (1.0 - sig)).astype(BF16)
        return 0

    first = pl.ds(0, SIDE - 1)
    early, late = n_tiles // 2, n_tiles - 1

    phase("backward1")
    lax.fori_loop(0, early, backward_step, 0)

    phase("rs1_wait")
    arrived("spread", spread_in)
    arrived("cross_x", cross_x)
    phase("rs1_sum")

    def first_sum(p, t_ref):
        summed = gsum[p, chunk_of(mine[p]), :]
        for k in range(SIDE - 1):
            summed = summed + spread_in[p, k].astype(F32)
        crossed = cross_sum[p, x]
        for k in range(CHIPS - 1):
            crossed = crossed + cross_x[p, k]
        for c, total in enumerate((summed, crossed)):
            for r in range(part // 8):
                t_ref[2 * r + c] = total[r * 8 : r * 8 + 8, :] * scale

    first_sum(0, t_a)
    first_sum(1, t_b)
    for k in ORDER:
        send(t_a.at[(z + k) % SIDE], rt_a.at[k - 1], at_z[k], "second_a", "tiles")
        send(t_b.at[(y + k) % SIDE], rt_b.at[k - 1], at_y[k], "second_b", "tiles")

    phase("backward2")
    lax.fori_loop(early, late, backward_step, 0)

    phase("small_0")
    arrived("small_0", sm_in)
    total = sm_all[dp]
    for k in range(n_dp - 1):
        total = total + sm_in[k]
    sm_ya[y] = total[:2]
    sm_zb[z] = total[2:]
    for k in ORDER:
        send(sm_ya.at[y], sm_ya.at[y], at_y[k], "small_1a", "small_1")
        send(sm_zb.at[z], sm_zb.at[z], at_z[k], "small_1b", "small_1")

    phase("backward3")
    lax.fori_loop(late, n_tiles, backward_step, 0)

    phase("rs2_wait")
    arrived("second_a", rt_a)
    arrived("second_b", rt_b)
    fin_a[y, z] = t_a[z] + added([rt_a[k] for k in range(SIDE - 1)])
    fin_b[z, y] = t_b[y] + added([rt_b[k] for k in range(SIDE - 1)])
    for k in ORDER:
        send(fin_a.at[y, z], fin_a.at[y, z], at_z[k], ("along_a", k), "tiles")
        send(fin_b.at[z, y], fin_b.at[z, y], at_y[k], ("along_b", k), "tiles")

    def pass_on(a_z, b_y):
        for k in ORDER:
            send(fin_a.at[y, a_z], fin_a.at[y, a_z], at_y[k], "across_a", "across_a")
            send(fin_b.at[z, b_y], fin_b.at[z, b_y], at_z[k], "across_b", "across_b")

    pass_on(z, y)

    phase("small_1")
    arrived("small_1a", sm_ya.at[first])
    arrived("small_1b", sm_zb.at[first])
    sm_za[z] = added([sm_ya[k] for k in range(SIDE)])
    sm_yb[y] = added([sm_zb[k] for k in range(SIDE)])
    for k in ORDER:
        send(sm_za.at[z], sm_za.at[z], at_z[k], "small_2a", "small_2")
        send(sm_yb.at[y], sm_yb.at[y], at_y[k], "small_2b", "small_2")

    phase("ag_pass")
    for k in NEAR_FIRST:
        arrived(("along_a", k), rt_a.at[0])
        arrived(("along_b", k), rt_b.at[0])
        pass_on((z + SIDE - k) % SIDE, (y + SIDE - k) % SIDE)

    phase("small_2")
    arrived("small_2a", sm_za.at[first])
    arrived("small_2b", sm_yb.at[first])
    sm_fin[dp, :2] = added([sm_za[k] for k in range(SIDE)])
    sm_fin[dp, 2:] = added([sm_yb[k] for k in range(SIDE)])
    for k in range(1, n_dp):
        send(sm_fin.at[dp], sm_fin.at[dp], at_dp[k], "small_3", "small_3")

    phase("ag2_wait")
    arrived("across_a", fin_a.at[first])
    arrived("across_b", fin_b.at[first])
    phase("assemble")
    for r in range(SIDE):
        for t in range(SIDE):
            line = slice(r * part + (t // 2) * 8, r * part + (t // 2) * 8 + 8)
            gw_ref[line, lanes(2 * (t % 2))] = fin_a[r, t]
            gw_ref[line, lanes(2 * (t % 2) + 1)] = fin_b[r, t]

    phase("small_3")
    arrived("small_3", sm_fin.at[pl.ds(0, n_dp - 1)])
    for t in range(blocks * per_block):
        cb, rb = t // per_block, t % per_block
        tile = sm_fin[t // OWN_TILES, t % OWN_TILES]
        for first_row, count, out in (
            (0, n_taps, taps_ref), (n_taps, 1, grad_gain), (n_taps + 1, 1, grad_shift)
        ):
            low, high = max(first_row, rb * 8), min(first_row + count, rb * 8 + 8)
            if low < high:
                out[low - first_row : high - first_row, lanes(cb)] = tile[low - rb * 8 : high - rb * 8]
    phase("send_wait")
    left("w", wfull.at[pl.ds(0, 7 * features), :])
    left("cot", cotp)
    left("act", actp)
    left("halo", halo)
    left("next", halo_next)
    left("next_cot", next_rows)
    left("far", far_in)
    left("opp", opp_in)
    left("near", near_in)
    left("spread", spread_in)
    left("cross", cross_in)
    left("cross_x", cross_x)
    left("tiles", fin_a.at[first, pl.ds(0, 4)])
    left("across_a", fin_a.at[first])
    left("across_b", fin_b.at[first])
    for i in range(4):
        left(f"small_{i}", sm_in)
    phase(None)
    assert len(send_ids) == SEND_SEMS and len(receive_ids) == RECEIVE_SEMS


def hand_out(*refs):
    sources, targets, sems = refs[:6], refs[6:12], refs[12]
    copies = [
        pltpu.make_async_copy(a, b, sems.at[i]) for i, (a, b) in enumerate(zip(sources, targets))
    ]
    for copy in copies:
        copy.start()
    for copy in copies:
        copy.wait()


def per_device(count, glu_value, glu_gate, cotangent, conv_weight, norm_gain, norm_shift, out_weight):
    value, gate, cot = glu_value[0], glu_gate[0], cotangent[0]
    rows, channels = value.shape
    n_taps = conv_weight.shape[0]
    features = out_weight.shape[0]
    blocks = channels // LANES
    part = features // SIDE
    n_dp = 2 * CHIPS
    scale = 1.0 / math.sqrt(rows * count)
    hbm = pl.BlockSpec(memory_space=pltpu.HBM)
    anywhere = pl.BlockSpec(memory_space=pl.ANY)
    vmem = pl.BlockSpec(memory_space=pltpu.VMEM)
    shape = jax.ShapeDtypeStruct
    buffer = pltpu.VMEM
    tile = (8, LANES)
    piece = (2, features, LANES)
    outs = pl.pallas_call(
        functools.partial(kernel, scale),
        out_shape=[
            pltpu.VMEM((rows, channels), BF16),
            pltpu.VMEM((rows, channels), BF16),
            pltpu.VMEM((features, channels), F32),
            pltpu.VMEM((n_taps, channels), F32),
            pltpu.VMEM((1, channels), F32),
            pltpu.VMEM((1, channels), F32),
        ],
        in_specs=[hbm] * 7,
        out_specs=[vmem] * 6,
        scratch_shapes=[
            buffer((rows, channels), BF16),
            buffer((rows, channels), BF16),
            buffer((rows + HALO, cot.shape[1]), BF16),
            buffer((n_taps, channels), F32),
            buffer((1, channels), F32),
            buffer((1, channels), F32),
            buffer((features, channels), BF16),
            buffer((2, HALO, channels), BF16),
            buffer((2, HALO, channels), BF16),
            buffer((blocks, rows + 2 * HALO, LANES), F32),
            buffer((blocks, rows + HALO, LANES), F32),
            buffer((rows + HALO, LANES), F32),
            buffer((blocks, rows + HALO, LANES), F32),
            buffer((rows + HALO, channels), F32),
            buffer((blocks, rows + HALO, LANES), F32),
            buffer((rows, channels), BF16),
            buffer((rows, channels), BF16),
            buffer((CHIPS, rows, features), BF16),
            buffer((n_dp * features, channels), BF16),
            buffer(piece, BF16),
            buffer(piece, BF16),
            buffer(piece, BF16),
            buffer(piece, BF16),
            buffer(piece, BF16),
            buffer(piece, BF16),
            buffer(piece, F32),
            buffer((2, features, channels), F32),
            buffer(piece, F32),
            buffer((2, CHIPS, features, LANES), BF16),
            buffer((2, CHIPS, features, LANES), F32),
            buffer((2, SIDE - 1, CHIPS, part, LANES), BF16),
            buffer((2, CHIPS, part, LANES), F32),
            buffer((2, CHIPS - 1, part, LANES), F32),
            buffer(piece, BF16),
            buffer((2, SIDE - 1, part, LANES), BF16),
            buffer((SIDE, *tile), F32),
            buffer((SIDE, *tile), F32),
            buffer((SIDE - 1, *tile), F32),
            buffer((SIDE - 1, *tile), F32),
            buffer((SIDE, SIDE, *tile), F32),
            buffer((SIDE, SIDE, *tile), F32),
            buffer((blocks, n_taps, *tile), F32),
            buffer((2, blocks, *tile), F32),
            buffer((n_dp, OWN_TILES, *tile), F32),
            buffer((n_dp - 1, OWN_TILES, *tile), F32),
            buffer((SIDE, 2, *tile), F32),
            buffer((SIDE, OWN_TILES - 2, *tile), F32),
            buffer((SIDE, 2, *tile), F32),
            buffer((SIDE, OWN_TILES - 2, *tile), F32),
            buffer((n_dp, OWN_TILES, *tile), F32),
            pltpu.SemaphoreType.DMA((SEND_SEMS,)),
            pltpu.SemaphoreType.DMA((RECEIVE_SEMS,)),
            pltpu.SemaphoreType.DMA((7,)),
        ],
        compiler_params=pltpu.CompilerParams(
            collective_id=0, has_side_effects=True, vmem_limit_bytes=62 * 2**20
        ),
        name="backward",
    )(value, gate, cot, conv_weight, norm_gain[None], norm_shift[None], out_weight)
    grad_value, grad_gate, grad_weight, grad_taps, grad_gain, grad_shift = pl.pallas_call(
        hand_out,
        out_shape=[
            shape((rows, channels), BF16),
            shape((rows, channels), BF16),
            shape((features, channels), F32),
            shape((n_taps, channels), F32),
            shape((1, channels), F32),
            shape((1, channels), F32),
        ],
        in_specs=[vmem] * 6,
        out_specs=[anywhere] * 6,
        scratch_shapes=[pltpu.SemaphoreType.DMA((6,))],
        compiler_params=pltpu.CompilerParams(vmem_limit_bytes=16 * 2**20),
        name="hand_out",
    )(*outs)
    return (
        grad_value[None], grad_gate[None], grad_weight,
        grad_taps, grad_gain.reshape(channels), grad_shift.reshape(channels),
    )


def solution(mesh):
    return jax.shard_map(
        functools.partial(per_device, mesh.size),
        mesh=mesh,
        in_specs=(
            P("dp", "sp", None), P("dp", "sp", None), P("dp", "sp", None),
            P(), P(), P(), P("dp", None),
        ),
        out_specs=(P("dp", "sp", None), P("dp", "sp", None), P("dp", None), P(), P(), P()),
        check_vma=False,
    )
```

time: 65.4 us -> 56.3 us (0.86)
  Pallas kernels: 64.6 us -> 55.5 us
    pallas_call x1, Pallas kernels: 63.3 us -> 54.3 us  [per_device(): pl.pallas_call(functools.partial(kernel, scale), out_shape=[pltpu.VMEM((r...]
where the time goes in v3:
time: 56.3 us; the launch traced here: 56.1 us
  Pallas kernels  55.5 us (99%)
  between operations  0.64 us (1%)
    pallas_call x1, Pallas kernels, per_device(): pl.pallas_call(functools.partial(kernel, scale), out_shape=[pltpu.VMEM((r...  54.3 us
    pallas_call x1, Pallas kernels, per_device(): pl.pallas_call(hand_out, out_shape=[shape((rows, channels), BF16), shape(...  1.21 us

profile of v3, /device:TPU:1, one launch (start us, length us, event | category | flops | bytes accessed | tf_op | source)
XLA Modules:
  0.0 56.1 jit_solution(8578378956740961212)
XLA Ops:
  0.6 54.3 %backward.1 = (bf16[512,512]{1,0:T(8,128)(2,1)S(1)}, bf16[512,512]{1,0:T(8,128)(2,1)S(1)}, f32[256,512]{1,0:T(8,128)S(1)}, f32[31,512]{1,0:T(8,128)S(1)}, f32[1,512]{1,0:T(1,128)S(1)}, /*index=5*/f32[1,512]{1,0:T(1,128)S(1)}) custom-call(bf16[512,512]{1,0:T(8,128)(2,1)} %bitcast.10, bf16[512,512]{1,0:T(8,128)(2,1)} %bitcast.11, bf16[512,2048]{1,0:T(8,128)(2,1)} %bitcast.9, ...), custom_call_target="tpu_custom_call" | custom-call | tf_op jit(solution)/shard_map/backward/pallas_call | solution.py:601
  54.9 1.2 %hand_out.1 = (bf16[512,512]{1,0:T(8,128)(2,1)}, bf16[512,512]{1,0:T(8,128)(2,1)}, f32[256,512]{1,0:T(8,128)}, f32[31,512]{1,0:T(8,128)}, f32[1,512]{1,0:T(1,128)}, /*index=5*/f32[1,512]{1,0:T(1,128)}) custom-call(bf16[512,512]{1,0:T(8,128)(2,1)S(1)} %get-tuple-element.18.refs_0_, bf16[512,512]{1,0:T(8,128)(2,1)S(1)} %get-tuple-element.19.refs_1_, ...), custom_call_target="tpu_custom_call" | custom-call | tf_op jit(solution)/shard_map/hand_out/pallas_call | solution.py:673

commit v4 on v3

--- a/solution.py
+++ b/solution.py
@@ -88,7 +88,8 @@
         return {"sp": sp, "dp": 2 * where + core}
 
     barrier = pltpu.get_barrier_semaphore()
-    peers = [after, before, *at_dp.values(), *at_y.values(), *at_z.values()]
+    peers = [at[k] for k in ORDER for at in (at_y, at_z)]
+    peers += [after, before, *at_dp.values()]
     for peer in peers:
         pl.semaphore_signal(barrier, inc=1, device_id=peer, device_id_type=MESH)
 
@@ -143,55 +144,6 @@
     phase("loads2")
     for copy in loads[2:]:
         copy.wait()
-    phase("barrier")
-    pl.semaphore_wait(barrier, len(peers))
-    phase("issue")
-
-    send(v_ref.at[pl.ds(rows - HALO, HALO), :], halo.at[0], after, "halo", "halo")
-    send(g_ref.at[pl.ds(rows - HALO, HALO), :], halo.at[1], after, "halo", "halo")
-    send(v_ref.at[pl.ds(0, HALO), :], halo_next.at[0], before, "next", "next")
-    send(g_ref.at[pl.ds(0, HALO), :], halo_next.at[1], before, "next", "next")
-    next_rows = cot_ref.at[pl.ds(rows, HALO), :]
-
-    def columns(owner_x, owner_core):
-        return pl.ds(pl.multiple_of((2 * owner_x + owner_core) * features, features), features)
-
-    def shard(owner_x, owner_core):
-        return wfull.at[columns(owner_x, owner_core), :]
-
-    parity = (y + z) % 2
-    half_rows, quarter_rows = features // 2, features // 8
-
-    def shard_half(owner_x, which):
-        first = (2 * owner_x + core) * features + which * half_rows
-        return wfull.at[pl.ds(pl.multiple_of(first, half_rows), half_rows), :]
-
-    def shard_quarter(owner_x, i):
-        first = (2 * owner_x + core) * features + parity * half_rows + i * quarter_rows
-        return wfull.at[pl.ds(pl.multiple_of(first, quarter_rows), quarter_rows), :]
-
-    own_half = ow_ref.at[pl.ds(pl.multiple_of(parity * half_rows, half_rows), half_rows), :]
-    send(own_half, shard_half(x, parity), chip(ahead_x), "ahead", "w")
-    send(own_half, shard_half(x, parity), chip(behind_x), "behind", "w")
-    send(ow_ref, shard(x, core), other, "pair_w", "w")
-    around = (at_y[1], at_y[SIDE - 1], at_z[1], at_z[SIDE - 1])
-
-    def pass_half(owner_x, name):
-        half_in = shard_half(owner_x, parity)
-        for i in range(4):
-            quarter = shard_quarter(owner_x, i)
-            send(quarter, quarter, around[i], name, "w")
-        send(half_in, half_in, other, "pair_w", "w")
-
-    def pass_rest(owner_x, name):
-        rest = shard_half(owner_x, 1 - parity)
-        arrived(name, rest)
-        send(rest, rest, other, "pair_w", "w")
-
-    for k in range(CHIPS):
-        send(cot_ref.at[pl.ds(0, rows), columns(k, 1 - core)], cotp.at[k], other, "cot", "cot")
-    wfull[columns(x, core), :] = ow_ref[...]
-
     def conv_rows(base, size):
         for cb in range(blocks):
             acc = jnp.zeros((size, LANES), F32)
@@ -227,13 +179,59 @@
         over_tiles(first_tile, last_tile, conv_rows)
         over_tiles(first_tile, last_tile, norm_rows)
 
+    n_tiles = rows // TILE
+    phase("forward_a")
+    forward(1, 3)
+    phase("barrier")
+    pl.semaphore_wait(barrier, len(peers))
+    phase("issue")
+
+    send(v_ref.at[pl.ds(rows - HALO, HALO), :], halo.at[0], after, "halo", "halo")
+    send(g_ref.at[pl.ds(rows - HALO, HALO), :], halo.at[1], after, "halo", "halo")
+    send(v_ref.at[pl.ds(0, HALO), :], halo_next.at[0], before, "next", "next")
+    send(g_ref.at[pl.ds(0, HALO), :], halo_next.at[1], before, "next", "next")
+    next_rows = cot_ref.at[pl.ds(rows, HALO), :]
+
+    def columns(owner_x, owner_core):
+        return pl.ds(pl.multiple_of((2 * owner_x + owner_core) * features, features), features)
+
+    def shard(owner_x, owner_core):
+        return wfull.at[columns(owner_x, owner_core), :]
+
+    half_rows = features // 2
+
+    def shard_half(owner_x, which):
+        first = (2 * owner_x + core) * features + which * half_rows
+        return wfull.at[pl.ds(pl.multiple_of(first, half_rows), half_rows), :]
+
+    for h in range(2):
+        own_half = ow_ref.at[pl.ds(h * half_rows, half_rows), :]
+        send(own_half, shard_half(x, h), chip(ahead_x), ("ahead", h), "w")
+        send(own_half, shard_half(x, h), chip(behind_x), ("behind", h), "w")
+    send(ow_ref, shard(x, core), other, "pair_w", "w")
+
+    def to_other(half):
+        send(half, half, other, "pair_w", "w")
+
+    def pass_half(h):
+        half = shard_half(behind_x, h)
+        arrived(("ahead", h), half)
+        send(half, half, chip(ahead_x), ("far_w", h), "w")
+        to_other(half)
+        half = shard_half(ahead_x, h)
+        arrived(("behind", h), half)
+        to_other(half)
+
+    for k in range(CHIPS):
+        send(cot_ref.at[pl.ds(0, rows), columns(k, 1 - core)], cotp.at[k], other, "cot", "cot")
+    wfull[columns(x, core), :] = ow_ref[...]
+
     def send_act(first, last):
         lines = pl.ds(first * TILE, (last - first) * TILE)
         send(act.at[lines, :], actp.at[lines, :], other, "act", "act")
 
-    n_tiles = rows // TILE
     phase("forward")
-    forward(1, n_tiles // 2)
+    forward(3, n_tiles // 2)
     send_act(1, n_tiles // 2)
     forward(n_tiles // 2, n_tiles)
     send_act(n_tiles // 2, n_tiles)
@@ -249,12 +247,7 @@
     send_act(0, 1)
 
     phase("w_wait1")
-    arrived("ahead", shard_half(behind_x, parity))
-    passed = shard_half(behind_x, parity)
-    send(passed, passed, chip(ahead_x), "far", "w")
-    pass_half(behind_x, "quarters_behind")
-    arrived("behind", shard_half(ahead_x, parity))
-    pass_half(ahead_x, "quarters_ahead")
+    pass_half(0)
     send(cot_ref.at[pl.ds(0, HALO), :], next_rows, before, "next_cot", "next_cot")
 
     phase("forward_next")
@@ -307,24 +300,19 @@
         near_st[p] = (near_own[p] + far_in[p].astype(F32)).astype(BF16)
         send(near_st.at[p], near_in.at[p], chip(ahead_x), ("near", p), "near")
 
-    phase("w_rest0")
-    pass_rest(behind_x, "quarters_behind")
-    passed_rest = shard_half(behind_x, 1 - parity)
-    send(passed_rest, passed_rest, chip(ahead_x), "far_rest", "w")
-    phase("w_rest1")
-    pass_rest(ahead_x, "quarters_ahead")
     for k in ORDER:
         for p in crossing:
             source = cross_st.at[p - 2, :, chunk_of((mine[p] + k) % SIDE), :]
             send(source, cross_in.at[p - 2, k - 1], around_all[p][k], "cross", "cross")
-    phase("w_wait2")
-    for name, which in (("far", parity), ("far_rest", 1 - parity)):
-        far_half = shard_half(far_x, which)
-        arrived(name, far_half)
-        send(far_half, far_half, other, "pair_w", "w")
+    phase("w_wait1b")
+    pass_half(1)
     phase("relay0")
     relay(0)
     relay(1)
+    phase("w_wait2")
+    for h in range(2):
+        arrived(("far_w", h), shard_half(far_x, h))
+        to_other(shard_half(far_x, h))
     phase("w_wait4")
     arrived("pair_w", wfull.at[pl.ds(0, CHIPS * features), :])
 
@@ -393,8 +381,6 @@
                 taps[cb, j] = taps[cb, j] + fold(own * shifted)
         return 0
 
-    phase("taps1")
-    lax.fori_loop(0, n_tiles // 2, taps_step, 0)
     phase("cross_wait")
     arrived("cross", cross_in)
     for p in crossing:
@@ -406,6 +392,8 @@
         for k in (2, 1, 3):
             to = (x + k) % CHIPS
             send(cross_sum.at[p - 2, to], cross_x.at[p - 2, k - 1], chip(to), "cross_x", "cross_x")
+    phase("taps1")
+    lax.fori_loop(0, n_tiles // 2, taps_step, 0)
     phase("taps2")
     lax.fori_loop(n_tiles // 2, n_tiles, taps_step, 0)
 

time: 56.3 us -> 55.5 us (0.986)
  Pallas kernels: 55.5 us -> 54.7 us
    pallas_call x1, Pallas kernels: 54.3 us -> 53.5 us  [per_device(): pl.pallas_call(functools.partial(kernel, scale), out_shape=[pltpu.VMEM((r...]
where the time goes in v4:
time: 55.5 us; the launch traced here: 55.4 us
  Pallas kernels  54.7 us (99%)
  between operations  0.64 us (1%)
    pallas_call x1, Pallas kernels, per_device(): pl.pallas_call(functools.partial(kernel, scale), out_shape=[pltpu.VMEM((r...  53.5 us
    pallas_call x1, Pallas kernels, per_device(): pl.pallas_call(hand_out, out_shape=[shape((rows, channels), BF16), shape(...  1.21 us

profile of v4, /device:TPU:1, one launch (start us, length us, event | category | flops | bytes accessed | tf_op | source)
XLA Modules:
  0.0 55.4 jit_solution(13285716513224482964)
XLA Ops:
  0.6 53.5 %backward.1 = (bf16[512,512]{1,0:T(8,128)(2,1)S(1)}, bf16[512,512]{1,0:T(8,128)(2,1)S(1)}, f32[256,512]{1,0:T(8,128)S(1)}, f32[31,512]{1,0:T(8,128)S(1)}, f32[1,512]{1,0:T(1,128)S(1)}, /*index=5*/f32[1,512]{1,0:T(1,128)S(1)}) custom-call(bf16[512,512]{1,0:T(8,128)(2,1)} %bitcast.10, bf16[512,512]{1,0:T(8,128)(2,1)} %bitcast.11, bf16[512,2048]{1,0:T(8,128)(2,1)} %bitcast.9, ...), custom_call_target="tpu_custom_call" | custom-call | tf_op jit(solution)/shard_map/backward/pallas_call | solution.py:589
  54.2 1.2 %hand_out.1 = (bf16[512,512]{1,0:T(8,128)(2,1)}, bf16[512,512]{1,0:T(8,128)(2,1)}, f32[256,512]{1,0:T(8,128)}, f32[31,512]{1,0:T(8,128)}, f32[1,512]{1,0:T(1,128)}, /*index=5*/f32[1,512]{1,0:T(1,128)}) custom-call(bf16[512,512]{1,0:T(8,128)(2,1)S(1)} %get-tuple-element.18.refs_0_, bf16[512,512]{1,0:T(8,128)(2,1)S(1)} %get-tuple-element.19.refs_1_, ...), custom_call_target="tpu_custom_call" | custom-call | tf_op jit(solution)/shard_map/hand_out/pallas_call | solution.py:661
